TPU v7x, 512 devices: a whole 4x4x16 slice. The times are simulated.
512 devices in a mesh: sp: 16 (over z), dp: 32 (over y, x, core).
Axes of the slice: x: 4, y: 4, z: 16, core: 2. Of those that a mesh axis runs over, the one named last changes fastest.
Arguments:
- inputs: bfloat16 [32, 2048, 2048], P('dp', 'sp'), may hold values from -6 to 6
- queries: bfloat16 [32, 2048, 1024], P('dp', 'sp'), may hold values from -6 to 6
- keys: bfloat16 [32, 2048, 1024], P('dp', 'sp'), may hold values from -1.5 to 1.5
- values: bfloat16 [32, 2048, 1024], P('dp', 'sp'), may hold values from -6 to 6
- log_decay: bfloat16 [32, 2048, 1024], P('dp', 'sp'), may hold values from -0.1 to 0, as said below
- cotangent: bfloat16 [32, 2048, 1024], P('dp', 'sp'), may hold values from -0.59765625 to 0.59765625
- value_weight: bfloat16 [2048, 1024], P('dp'), may hold values from -0.125 to 0.125
Outputs:
- grad_queries: bfloat16 [32, 2048, 1024], P('dp', 'sp')
- grad_keys: bfloat16 [32, 2048, 1024], P('dp', 'sp')
- grad_decay: bfloat16 [32, 2048, 1024], P('dp', 'sp')
- grad_inputs: bfloat16 [32, 2048, 2048], P('dp', 'sp')
- grad_weight: float32 [2048, 1024], P('dp')
Inputs may be any that keep to these rules, and one draw needn't show every extreme that they name: `log_decay`: the log decays are negative; per key channel and sequence they differ between positions.
All inputs are finite; a program needn't handle non-finite values.
Results may differ from a plain program's by a relative error of at most 0.015.
Values may be sent and summed in bfloat16 or wider, within the bound.
A program may use at most 128 MiB of HBM per device.

v0:
```python
import jax
import jax.numpy as jnp
from jax import lax
from jax.sharding import PartitionSpec as P

HEADS = 16
HEAD_DIM = 64
BLOCK = 128


def in_blocks(x, dim, length):
    before, after = (x.shape[:dim], x.shape[dim + 1 :])
    return jnp.moveaxis(x.reshape(*before, length, -1, *after), dim, 0)


def sent_and_summed(x, axis, dim):
    length = lax.axis_size(axis)
    tiles = lax.all_to_all(in_blocks(x, dim, length), axis, 0, 0, tiled=True)
    return jnp.sum(tiles, axis=0)


def sent_to_all(x, axis):
    length = lax.axis_size(axis)
    return lax.all_to_all(jnp.broadcast_to(x[None], (length, *x.shape)), axis, 0, 0, tiled=True)


def laid_out(tiles, dim):
    tiles = jnp.moveaxis(tiles, 0, dim)
    dims = tiles.shape
    return tiles.reshape(*dims[:dim], dims[dim] * dims[dim + 1], *dims[dim + 2 :])


def gathered_copies(x, axis, dim):
    tiles = sent_to_all(x, axis)
    return laid_out(tiles, dim)


def combine(earlier, later):
    first_decay, first_state = earlier
    second_decay, second_state = later
    return (first_decay * second_decay, second_decay[..., None] * first_state + second_state)


def carry_scan(decays, updates):
    return lax.associative_scan(combine, (decays, updates), axis=0)[1]


def to_blocks(rows, num_blocks):
    length, groups, width = rows.shape
    return jnp.transpose(
        rows.astype(jnp.float32).reshape(num_blocks, BLOCK, groups, width), (0, 2, 3, 1)
    )


def mixing(query_rows, key_rows, value_rows, gate_rows):
    length, groups, key_width = query_rows.shape
    value_width = value_rows.shape[2]
    num_blocks = length // BLOCK
    scaled_query = to_blocks(query_rows, num_blocks) * HEAD_DIM ** (-0.5)
    key_float = to_blocks(key_rows, num_blocks)
    value_float = to_blocks(value_rows, num_blocks)
    gate_float = to_blocks(gate_rows, num_blocks)
    running = jnp.cumsum(gate_float, axis=3)
    exclusive = running - gate_float
    block_end = running[..., -1]
    lower_mask = jnp.tril(jnp.ones((BLOCK, BLOCK), jnp.float32))
    upper_mask = lower_mask.T
    query_fwd = scaled_query * jnp.exp(running)
    key_fwd = key_float * jnp.exp(-running)
    scores_fwd = jnp.einsum("ngcr,ngcs->ngrs", query_fwd, key_fwd) * lower_mask
    key_end = key_float * jnp.exp(block_end[..., None] - running)
    states = carry_scan(jnp.exp(block_end), jnp.einsum("ngcs,ngvs->ngcv", key_end, value_float))
    before = jnp.concatenate([jnp.zeros_like(states[:1]), states[:-1]], axis=0)
    out_fwd = jnp.einsum("ngrs,ngvs->ngvr", scores_fwd, value_float) + jnp.einsum(
        "ngcr,ngcv->ngvr", query_fwd, before
    )
    query_bwd = scaled_query * jnp.exp(-exclusive)
    key_bwd = key_float * jnp.exp(exclusive)
    scores_bwd = jnp.einsum("ngcr,ngcs->ngrs", query_bwd, key_bwd) * upper_mask
    rights = jnp.flip(
        carry_scan(
            jnp.flip(jnp.exp(block_end), 0),
            jnp.flip(jnp.einsum("ngcs,ngvs->ngcv", key_bwd, value_float), 0),
        ),
        0,
    )
    after = jnp.concatenate([rights[1:], jnp.zeros_like(rights[:1])], axis=0)
    query_read = scaled_query * jnp.exp(block_end[..., None] - exclusive)
    out_bwd = jnp.einsum("ngrs,ngvs->ngvr", scores_bwd, value_float) + jnp.einsum(
        "ngcr,ngcv->ngvr", query_read, after
    )
    total = out_fwd + out_bwd
    return jnp.transpose(total, (0, 3, 1, 2)).reshape(length, groups, value_width)


def per_device(inputs, queries, keys, values, log_decay, cotangent, value_weight):
    local_tokens = inputs.shape[1]
    seq_devices = lax.axis_size("sp")
    head_share = HEADS // seq_devices
    half_width = HEAD_DIM // 2

    def by_head(array):
        return array[0].reshape(local_tokens, seq_devices, head_share, HEAD_DIM)

    packed = jnp.concatenate(
        [by_head(queries), by_head(keys), by_head(log_decay), by_head(values), by_head(cotangent)],
        axis=3,
    )
    head_rows = lax.all_to_all(packed, "sp", split_axis=1, concat_axis=0, tiled=True)[:, 0]
    length = head_rows.shape[0]
    head_count = head_rows.shape[1]

    def groups_of(array):
        return array.reshape(length, 2 * head_count, half_width)

    def spread(array):
        return jnp.broadcast_to(array[:, :, None, :], (length, head_count, 2, HEAD_DIM)).reshape(
            length, 2 * head_count, HEAD_DIM
        )

    query_rows = groups_of(head_rows[..., :HEAD_DIM])
    key_rows = groups_of(head_rows[..., HEAD_DIM : 2 * HEAD_DIM])
    gate_rows = groups_of(head_rows[..., 2 * HEAD_DIM : 3 * HEAD_DIM])
    value_rows = spread(head_rows[..., 3 * HEAD_DIM : 4 * HEAD_DIM])
    upstream = spread(head_rows[..., 4 * HEAD_DIM :])
    _, pullback = jax.vjp(mixing, query_rows, key_rows, value_rows, gate_rows)
    grad_q, grad_k, grad_v, grad_g = pullback(upstream.astype(jnp.float32))
    value_sum = jnp.sum(grad_v.astype(jnp.float32).reshape(length, head_count, 2, HEAD_DIM), axis=2)
    joined = jnp.concatenate(
        [
            grad_q.reshape(length, head_count, HEAD_DIM),
            grad_k.reshape(length, head_count, HEAD_DIM),
            grad_g.reshape(length, head_count, HEAD_DIM),
            value_sum.astype(jnp.bfloat16),
        ],
        axis=2,
    )
    grad_heads = joined[:, None]
    returned = lax.all_to_all(grad_heads, "sp", split_axis=0, concat_axis=1, tiled=True)
    token_grads = returned.reshape(local_tokens, HEADS, 4 * HEAD_DIM)
    grad_queries = token_grads[..., :HEAD_DIM].reshape(1, local_tokens, HEADS * HEAD_DIM)
    grad_keys = token_grads[..., HEAD_DIM : 2 * HEAD_DIM].reshape(1, local_tokens, HEADS * HEAD_DIM)
    grad_decay = token_grads[..., 2 * HEAD_DIM : 3 * HEAD_DIM].reshape(
        1, local_tokens, HEADS * HEAD_DIM
    )
    value_grad = token_grads[..., 3 * HEAD_DIM :].reshape(local_tokens, HEADS * HEAD_DIM)
    grad_inputs = lax.dot_general(
        value_grad,
        lax.all_gather(value_weight, "dp", axis=0, tiled=True),
        (((1,), (1,)), ((), ())),
        preferred_element_type=jnp.float32,
    ).astype(jnp.bfloat16)[None]
    head_values = grad_heads[:, 0, :, 3 * HEAD_DIM :].reshape(
        grad_heads.shape[0], head_share * HEAD_DIM
    )
    column_part = lax.dot_general(
        lax.all_gather(inputs, "sp", axis=1, tiled=True)[0],
        head_values,
        (((0,), (0,)), ((), ())),
        preferred_element_type=jnp.float32,
    )
    row_part = sent_and_summed(column_part, "dp", 0)
    grad_weight = gathered_copies(row_part, "sp", 1)
    return (grad_queries, grad_keys, grad_decay, grad_inputs, grad_weight)


def solution(mesh):
    return jax.shard_map(
        per_device,
        mesh=mesh,
        in_specs=(
            P("dp", "sp", None),
            P("dp", "sp", None),
            P("dp", "sp", None),
            P("dp", "sp", None),
            P("dp", "sp", None),
            P("dp", "sp", None),
            P("dp", None),
        ),
        out_specs=(
            P("dp", "sp", None),
            P("dp", "sp", None),
            P("dp", "sp", None),
            P("dp", "sp", None),
            P("dp", None),
        ),
        check_vma=False,
    )
```

profile of v0, /device:TPU:32, one launch (start us, length us, event | category | flops | bytes accessed | tf_op | source)
XLA Modules:
  0.0 514.5 jit_solution(9123862074791712167)
XLA Ops:
  15.5 15.2 %all-to-all-start = ((bf16[128,16,1,320]{0,3,2,1:T(8,128)(2,1)}), bf16[128,16,1,320]{0,3,2,1:T(8,128)(2,1)S(1)}, u32[]{:S(2)}, u32[]{:S(2)}) async-start(bf16[128,16,1,320]{0,3,2,1:T(8,128)(2,1)} %bitcast.5), calls=%async_computation | async-start | bytes 2621440 | tf_op jit(solution)/shard_map/all_to_all | solution.py:109
  32.7 72.9 %all-to-all-done = bf16[128,16,1,320]{0,3,2,1:T(8,128)(2,1)S(1)} async-done(((bf16[128,16,1,320]{0,3,2,1:T(8,128)(2,1)}), bf16[128,16,1,320]{0,3,2,1:T(8,128)(2,1)S(1)}, u32[]{:S(2)}, u32[]{:S(2)}) %all-to-all-start) | async-done | bytes 1310752 | tf_op jit(solution)/shard_map/all_to_all | solution.py:109
  108.1 9.2 %reduce_window_sum.26 = f32[16,2,32,128]{3,2,1,0:T(8,128)S(1)} reduce-window(f32[16,2,32,128]{3,2,1,0:T(8,128)S(1)} %bitcast.345, f32[]{:T(128)} %constant.15.clone.1), window={size=1x1x1x128 pad=0_0x0_0x0_0x127_0}, to_apply=%region_0.0 | reduce-window | flops 16646144 | bytes 1048580 | tf_op jit(solution)/shard_map/jvp(jit(cumsum))/reduce_window_sum | solution.py:63
  135.9 4.8 pad.303
  140.7 4.8 pad.304
  194.5 5.6 %pad.355 = f32[16,2,32,64]{3,2,1,0:T(8,128)} pad(f32[8,2,32,64]{3,2,1,0:T(8,128)S(1)} %get-tuple-element.34, f32[]{:T(128)} %constant.15.clone.1), padding=1_0_1x0_0_0x0_0_0x0_0_0 | pad | bytes 393220 | tf_op jit(solution)/shard_map/transpose(jvp())/pad | solution.py:45
  201.4 5.6 %pad.330 = f32[16,2,32,64]{3,2,1,0:T(8,128)} pad(f32[8,2,32,64]{3,2,1,0:T(8,128)S(1)} %get-tuple-element.28, f32[]{:T(128)} %constant.15.clone.1), padding=1_0_1x0_0_0x0_0_0x0_0_0 | pad | bytes 393220 | tf_op jit(solution)/shard_map/transpose(jvp())/pad | solution.py:45
  209.2 8.7 %pad.521 = f32[16,2,32,64]{3,2,1,0:T(8,128)} pad(f32[8,2,32,64]{3,2,1,0:T(8,128)} %add.235, f32[]{:T(128)} %constant.15.clone.1), padding=1_0_1x0_0_0x0_0_0x0_0_0 | pad | bytes 393220
  217.9 8.7 %pad.402 = f32[15,2,32,64]{3,2,1,0:T(8,128)} pad(f32[8,2,32,64]{3,2,1,0:T(8,128)} %get-tuple-element.127, f32[]{:T(128)} %constant.15.clone.1), padding=0_0_1x0_0_0x0_0_0x0_0_0 | pad | bytes 376836 | tf_op jit(solution)/shard_map/jvp()/slice | solution.py:73
  245.3 4.8 pad.296
  254.1 8.7 %pad.522 = f32[16,2,32,64]{3,2,1,0:T(8,128)} pad(f32[8,2,32,64]{3,2,1,0:T(8,128)} %add.224, f32[]{:T(128)} %constant.15.clone.1), padding=1_0_1x0_0_0x0_0_0x0_0_0 | pad | bytes 393220
  264.4 8.7 %pad.400 = f32[15,2,32,64]{3,2,1,0:T(8,128)} pad(f32[8,2,32,64]{3,2,1,0:T(8,128)} %pad_maximum_fusion.1, f32[]{:T(128)} %constant.15.clone.1), padding=0_0_1x0_0_0x0_0_0x0_0_0 | pad | bytes 376836 | tf_op jit(solution)/shard_map/jvp()/slice | solution.py:87
  276.7 8.7 %pad.356 = f32[16,2,32,64]{3,2,1,0:T(8,128)} pad(f32[8,2,32,64]{3,2,1,0:T(8,128)} %broadcast_multiply_fusion, f32[]{:T(128)} %constant.15.clone.1), padding=0_1_1x0_0_0x0_0_0x0_0_0 | pad | bytes 393220 | tf_op jit(solution)/shard_map/transpose(jvp())/pad | solution.py:45
  285.5 7.5 %pad.333 = f32[16,2,32,64]{3,2,1,0:T(8,128)} pad(f32[7,2,32,64]{3,2,1,0:T(8,128)} %get-tuple-element.61, f32[]{:T(128)} %constant.15.clone.1), padding=2_1_1x0_0_0x0_0_0x0_0_0 | pad | bytes 376836 | tf_op jit(solution)/shard_map/transpose(jvp())/pad | solution.py:45
  309.2 8.7 %pad.331 = f32[16,2,32,64]{3,2,1,0:T(8,128)} pad(f32[8,2,32,64]{3,2,1,0:T(8,128)} %broadcast_multiply_fusion.1, f32[]{:T(128)} %constant.15.clone.1), padding=0_1_1x0_0_0x0_0_0x0_0_0 | pad | bytes 393220 | tf_op jit(solution)/shard_map/transpose(jvp())/pad | solution.py:45
  317.9 7.5 %pad.308 = f32[16,2,32,64]{3,2,1,0:T(8,128)} pad(f32[7,2,32,64]{3,2,1,0:T(8,128)} %split.47, f32[]{:T(128)} %constant.15.clone.1), padding=2_1_1x0_0_0x0_0_0x0_0_0 | pad | bytes 376836 | tf_op jit(solution)/shard_map/transpose(jvp())/pad | solution.py:45
  338.9 40.5 %reduce_window_sum.28 = f32[16,2,32,128]{3,2,1,0:T(8,128)S(1)} reduce-window(f32[16,2,32,128]{3,2,1,0:T(8,128)} %get-tuple-element.125, f32[]{:T(128)} %constant.15.clone.1), window={size=1x1x1x128 pad=0_0x0_0x0_0x0_127}, to_apply=%region_17.18 | reduce-window | flops 16646144 | bytes 1048580 | tf_op jit(solution)/shard_map/transpose(jvp(jit(cumsum)))/reduce_window_sum | solution.py:63
  393.5 5.1 fusion.3
  401.1 7.2 %all-to-all-start.2 = ((f32[32,1,4096]{2,1,0:T(1,128)}), f32[32,1,4096]{2,1,0:T(1,128)S(1)}, u32[]{:S(2)}, u32[]{:S(2)}) async-start(f32[32,1,4096]{2,1,0:T(1,128)} %reshape.288), calls=%async_computation.2 | async-start | bytes 1048576 | tf_op jit(solution)/shard_map/all_to_all | solution.py:18
  411.4 8.5 %all-to-all-done.2 = f32[32,1,4096]{2,1,0:T(1,128)S(1)} async-done(((f32[32,1,4096]{2,1,0:T(1,128)}), f32[32,1,4096]{2,1,0:T(1,128)S(1)}, u32[]{:S(2)}, u32[]{:S(2)}) %all-to-all-start.2) | async-done | bytes 524320 | tf_op jit(solution)/shard_map/all_to_all | solution.py:18
  419.9 8.7 %all-to-all-start.1 = ((bf16[16,2,16384]{2,1,0:T(2,128)(2,1)}), bf16[16,2,16384]{2,1,0:T(2,128)(2,1)S(1)}, u32[]{:S(2)}, u32[]{:S(2)}) async-start(bf16[16,2,16384]{2,1,0:T(2,128)(2,1)} %reshape.286), calls=%async_computation.1 | async-start | bytes 2097152 | tf_op jit(solution)/shard_map/all_to_all | solution.py:139
  432.8 45.8 %all-to-all-done.1 = bf16[16,2,16384]{2,1,0:T(2,128)(2,1)S(1)} async-done(((bf16[16,2,16384]{2,1,0:T(2,128)(2,1)}), bf16[16,2,16384]{2,1,0:T(2,128)(2,1)S(1)}, u32[]{:S(2)}, u32[]{:S(2)}) %all-to-all-start.1) | async-done | bytes 1048608 | tf_op jit(solution)/shard_map/all_to_all | solution.py:139
  478.5 8.2 %all-to-all-start.3 = ((f32[16,1,4096]{2,1,0:T(1,128)}), f32[16,1,4096]{2,1,0:T(1,128)S(1)}, u32[]{:S(2)}, u32[]{:S(2)}) async-start(f32[16,1,4096]{2,1,0:T(1,128)} %reshape.290), calls=%async_computation.3 | async-start | bytes 524288 | tf_op jit(solution)/shard_map/all_to_all | solution.py:24
  496.5 8.5 %all-to-all-done.3 = f32[16,1,4096]{2,1,0:T(1,128)S(1)} async-done(((f32[16,1,4096]{2,1,0:T(1,128)}), f32[16,1,4096]{2,1,0:T(1,128)S(1)}, u32[]{:S(2)}, u32[]{:S(2)}) %all-to-all-start.3) | async-done | bytes 262176 | tf_op jit(solution)/shard_map/all_to_all | solution.py:24
  (429 shorter events, 176.1 us)
Async XLA Ops:
  7.2 386.3 %all-gather.5.cloned.1.call-start = ((), (), s32[]{:S(2)}) async-start(), calls=%async_computation.5 | async-start | bytes 8912896 | tf_op jit(solution)/shard_map/all_gather | solution.py:157
  15.5 90.1 %all-to-all-start = ((bf16[128,16,1,320]{0,3,2,1:T(8,128)(2,1)}), bf16[128,16,1,320]{0,3,2,1:T(8,128)(2,1)S(1)}, u32[]{:S(2)}, u32[]{:S(2)}) async-start(bf16[128,16,1,320]{0,3,2,1:T(8,128)(2,1)} %bitcast.5), calls=%async_computation | async-start | bytes 2621440 | tf_op jit(solution)/shard_map/all_to_all | solution.py:109
  30.7 461.3 %all-gather.3.cloned.1.call-start = ((), (), s32[]{:S(2)}) async-start(), calls=%async_computation.4 | async-start | bytes 4325376 | tf_op jit(solution)/shard_map/all_gather | solution.py:149
  107.3 70.0 %copy-start.9 = (f32[8,8,16,128]{3,2,1,0:T(8,128)}, f32[8,8,16,128]{3,2,1,0:T(8,128)S(1)}, u32[]{:S(2)}) copy-start(f32[8,8,16,128]{3,2,1,0:T(8,128)S(1)} %copy.167) | copy-start | bytes 1572868
  120.8 57.6 %copy-start.6 = (bf16[16,128,64]{1,2,0:T(8,128)(2,1)}, bf16[16,128,64]{1,2,0:T(8,128)(2,1)S(1)}, u32[]{:S(2)}) copy-start(bf16[16,128,64]{1,2,0:T(8,128)(2,1)S(1)} %copy.135) | copy-start | bytes 786436
  123.0 54.3 %copy-start = (f32[8,8,16,128]{3,2,1,0:T(8,128)}, f32[8,8,16,128]{3,2,1,0:T(8,128)S(1)}, u32[]{:S(2)}) copy-start(f32[8,8,16,128]{3,2,1,0:T(8,128)S(1)} %copy.166) | copy-start | bytes 1572868
  181.6 25.4 %copy-start.19 = (f32[7,2,32,64]{3,2,1,0:T(8,128)}, f32[7,2,32,64]{3,2,1,0:T(8,128)S(1)}, u32[]{:S(2)}) copy-start(f32[7,2,32,64]{3,2,1,0:T(8,128)S(1)} %split.60) | copy-start | bytes 344068
  207.7 19.0 %copy-start.96 = (f32[2,2,32]{2,1,0:T(2,128)S(1)}, f32[2,2,32]{2,1,0:T(2,128)}, u32[]{:S(2)}) copy-start(f32[2,2,32]{2,1,0:T(2,128)} %get-tuple-element.31) | copy-start | bytes 1540
  207.7 19.0 %copy-start.97 = (f32[2,32]{1,0:T(2,128)S(1)}, f32[2,32]{1,0:T(2,128)}, u32[]{:S(2)}) copy-start(f32[2,32]{1,0:T(2,128)} %get-tuple-element.83) | copy-start | bytes 772
  207.7 20.3 %copy-start.62 = (f32[8,2,32]{2,1,0:T(2,128)S(1)}, f32[8,2,32]{2,1,0:T(2,128)}, u32[]{:S(2)}) copy-start(f32[8,2,32]{2,1,0:T(2,128)} %copy-done.61) | copy-start | bytes 6148
  207.7 20.3 %copy-start.86 = (f32[4,2,32]{2,1,0:T(2,128)S(1)}, f32[4,2,32]{2,1,0:T(2,128)}, u32[]{:S(2)}) copy-start(f32[4,2,32]{2,1,0:T(2,128)} %get-tuple-element.29) | copy-start | bytes 3076
  207.7 22.8 %copy-start.87 = (f32[3,2,32]{2,1,0:T(2,128)S(1)}, f32[3,2,32]{2,1,0:T(2,128)}, u32[]{:S(2)}) copy-start(f32[3,2,32]{2,1,0:T(2,128)} %get-tuple-element.59) | copy-start | bytes 2308
  207.7 24.5 %copy-start.55 = (f32[8,2,32]{2,1,0:T(2,128)S(1)}, f32[8,2,32]{2,1,0:T(2,128)}, u32[]{:S(2)}) copy-start(f32[8,2,32]{2,1,0:T(2,128)} %copy-done.53) | copy-start | bytes 6148
  207.7 24.5 %copy-start.60 = (f32[8,2,32]{2,1,0:T(2,128)S(1)}, f32[8,2,32]{2,1,0:T(2,128)}, u32[]{:S(2)}) copy-start(f32[8,2,32]{2,1,0:T(2,128)} %copy-done.59) | copy-start | bytes 6148
  207.7 31.2 %slice-start.1 = ((f32[8,2,32,64]{3,2,1,0:T(8,128)}), f32[1,2,32,64]{3,2,1,0:T(8,128)S(1)}, s32[]{:S(2)}) async-start(f32[8,2,32,64]{3,2,1,0:T(8,128)} %copy-done.23), calls=%async_computation.7 | async-start | bytes 65536 | tf_op jit(solution)/shard_map/jvp()/slice | solution.py:45
  209.2 42.6 %copy-start.72 = (f32[7,2,32]{2,1,0:T(2,128)S(1)}, f32[7,2,32]{2,1,0:T(2,128)}, u32[]{:S(2)}) copy-start(f32[7,2,32]{2,1,0:T(2,128)} %copy-done.71) | copy-start | bytes 5380
  226.6 36.1 %slice-start = ((f32[16,2,32,64]{3,2,1,0:T(8,128)}), f32[1,2,32,64]{3,2,1,0:T(8,128)S(1)}, s32[]{:S(2)}) async-start(f32[16,2,32,64]{3,2,1,0:T(8,128)} %copy-done.20), calls=%async_computation.6 | async-start | bytes 65536 | tf_op jit(solution)/shard_map/jvp()/slice | solution.py:45
  264.4 28.6 %slice-start.2 = ((f32[8,2,32,64]{3,2,1,0:T(8,128)}), f32[1,2,32,64]{3,2,1,0:T(8,128)S(1)}, s32[]{:S(2)}) async-start(f32[8,2,32,64]{3,2,1,0:T(8,128)} %slice.367), calls=%async_computation.8 | async-start | bytes 65536 | tf_op jit(solution)/shard_map/transpose(jvp())/split | solution.py:45
  276.7 19.6 %copy-start.79 = (f32[8,2,32]{2,1,0:T(2,128)S(1)}, f32[8,2,32]{2,1,0:T(2,128)}, u32[]{:S(2)}) copy-start(f32[8,2,32]{2,1,0:T(2,128)} %get-tuple-element.97) | copy-start | bytes 6148
  276.7 22.5 %copy-start.78 = (f32[8,2,32]{2,1,0:T(2,128)S(1)}, f32[8,2,32]{2,1,0:T(2,128)}, u32[]{:S(2)}) copy-start(f32[8,2,32]{2,1,0:T(2,128)} %get-tuple-element.98) | copy-start | bytes 6148
  276.7 25.4 %copy-start.80 = (f32[7,2,32]{2,1,0:T(2,128)S(1)}, f32[7,2,32]{2,1,0:T(2,128)}, u32[]{:S(2)}) copy-start(f32[7,2,32]{2,1,0:T(2,128)} %get-tuple-element.54) | copy-start | bytes 5380
  401.1 18.8 %all-to-all-start.2 = ((f32[32,1,4096]{2,1,0:T(1,128)}), f32[32,1,4096]{2,1,0:T(1,128)S(1)}, u32[]{:S(2)}, u32[]{:S(2)}) async-start(f32[32,1,4096]{2,1,0:T(1,128)} %reshape.288), calls=%async_computation.2 | async-start | bytes 1048576 | tf_op jit(solution)/shard_map/all_to_all | solution.py:18
  419.9 58.6 %all-to-all-start.1 = ((bf16[16,2,16384]{2,1,0:T(2,128)(2,1)}), bf16[16,2,16384]{2,1,0:T(2,128)(2,1)S(1)}, u32[]{:S(2)}, u32[]{:S(2)}) async-start(bf16[16,2,16384]{2,1,0:T(2,128)(2,1)} %reshape.286), calls=%async_computation.1 | async-start | bytes 2097152 | tf_op jit(solution)/shard_map/all_to_all | solution.py:139
  478.5 26.5 %all-to-all-start.3 = ((f32[16,1,4096]{2,1,0:T(1,128)}), f32[16,1,4096]{2,1,0:T(1,128)S(1)}, u32[]{:S(2)}, u32[]{:S(2)}) async-start(f32[16,1,4096]{2,1,0:T(1,128)} %reshape.290), calls=%async_computation.3 | async-start | bytes 524288 | tf_op jit(solution)/shard_map/all_to_all | solution.py:24
  (87 other events, 367.9 us)
Sparse Core Ops, SparseCore 0:
  10.1 163.6 all-gather.4
  176.9 61.4 all-gather.2
where the time goes:
time: 524 us; the launch traced here: 515 us
  local copies, waits for them, and re-layouts  184 us (35%)
  waiting for transfers between devices  137 us (26%)
  other arithmetic  108 us (21%)
  starting transfers between devices  39.4 us (8%)
  matrix products  30.7 us (6%)
  between operations  15.7 us (3%)
    pad x46, local copies, waits for them, and re-layouts, carry_scan(): return lax.associative_scan(combine, (decays, updates), axis=0)[1]  105 us
    all_to_all x1, waiting for transfers between devices, per_device(): lax.all_to_all(packed, 'sp', split_axis=1, concat_axis=0, tiled=True)[:, 0]  72.9 us
    another operation x2, other arithmetic, mixing(): running = jnp.cumsum(gate_float, axis=3)  49.7 us
    all_to_all x1, waiting for transfers between devices, per_device(): lax.all_to_all(grad_heads, 'sp', split_axis=0, concat_axis=1, tiled=True)  45.8 us
    unnamed x226, local copies, waits for them, and re-layouts  38.6 us
    reduce_sum x14, other arithmetic, combine(): second_decay[..., None] * first_state + second_state  17.9 us
    all_to_all x1, starting transfers between devices, per_device(): lax.all_to_all(packed, 'sp', split_axis=1, concat_axis=0, tiled=True)[:, 0]  15.2 us
  transfers between devices with their start and end apart: 6, of which 4 were waited for; matrix products, arithmetic and copies ran while one was open for 61% of the time, Pallas kernels for 0%

commit v1 on v0

v1 whole, which is shorter than its diff:
```python
import functools

import jax
import jax.numpy as jnp
from jax import lax
from jax.experimental import pallas as pl
from jax.experimental.pallas import tpu as pltpu
from jax.sharding import PartitionSpec as P

MESH = pl.DeviceIdType.MESH
F32 = jnp.float32
BF16 = jnp.bfloat16
BLOCK = 128
WIDTH = 1024
HALF = WIDTH // 2
PAIRS = WIDTH // 128
CHUNKS = 2 * PAIRS
HEAD_DIM = 64


def nn(a, b):
    return lax.dot_general(a, b, (((1,), (0,)), ((), ())), preferred_element_type=F32)


def nt(a, b):
    return lax.dot_general(a, b, (((1,), (1,)), ((), ())), preferred_element_type=F32)


def tn(a, b):
    return lax.dot_general(a, b, (((0,), (0,)), ((), ())), preferred_element_type=F32)


def lanes(start, size):
    return pl.ds(pl.multiple_of(start, 128), size)


def kernel(
    nz, nq,
    q_ref, k_ref, v_ref, g_ref, cot_ref, x_ref, w_ref,
    dq_ref, dk_ref, dg_ref, gi_ref, gw_ref,
    run_s, end_s, qf_s, kf_s, qb_s, kb_s, loc_s, raw_s, send_s, recv_s,
    dqf_s, dqb_s, dkf_s, dkb_s, dv_s, dvb_s,
    wv_s, xg_s, dvg_s, part_s, pb_s, s2_s, acc_s, zb_s, zr_s, rb_s, gr_s,
    chain_ss, chain_rs, w0_ss, w0_rs, w_loc, w1_ss, w1_rs, w2_ss, w2_rs, w3_ss, w3_rs,
    x_ss, x_rs, dv_ss, dv_rs, s2_ss, s2_rs, zr_ss, zr_rs, za_ss, za_rs,
):
    z = lax.axis_index("sp")
    d = lax.axis_index("dp")
    c = lax.rem(d, 2)
    chip = lax.div(d, 2)
    xx = lax.rem(chip, nq)
    yy = lax.div(chip, nq)
    pa = xx * (1 - c) + yy * c
    pb = yy * (1 - c) + xx * c

    def chip_at(a, b):
        return (b * nq + a) * (1 - c) + (a * nq + b) * c

    def there(chip_id, core, at_z=None):
        return {"sp": z if at_z is None else at_z, "dp": chip_id * 2 + core}

    def turned(at, i, n):
        return lax.rem(at + i, n)

    barrier = pltpu.get_barrier_semaphore()
    greeted = 0
    for i in range(1, nq):
        for core in range(2):
            for other in (yy * nq + turned(xx, i, nq), turned(yy, i, nq) * nq + xx):
                pl.semaphore_signal(barrier, inc=1, device_id=there(other, core), device_id_type=MESH)
                greeted += 1
    pl.semaphore_signal(barrier, inc=1, device_id=there(chip, 1 - c), device_id_type=MESH)
    for step in (1, nz - 1):
        pl.semaphore_signal(
            barrier, inc=1, device_id=there(chip, c, turned(z, step, nz)), device_id_type=MESH
        )
    pl.semaphore_wait(barrier, greeted + 3)

    def remote(src, dst, ss, rs, device):
        return pltpu.make_async_remote_copy(
            src_ref=src, dst_ref=dst, send_sem=ss, recv_sem=rs, device_id=device, device_id_type=MESH
        )

    w_here = pltpu.make_async_copy(
        w_ref.at[:, lanes(c * HALF, HALF)],
        wv_s.at[c, chip, pl.ds(pl.multiple_of(c * 64, 64), 64), :],
        w_loc,
    )
    w_here.start()
    w0 = remote(
        w_ref.at[:, lanes((1 - c) * HALF, HALF)],
        wv_s.at[1 - c, chip, pl.ds(pl.multiple_of(c * 64, 64), 64), :],
        w0_ss, w0_rs, there(chip, 1 - c),
    )
    w0.start()

    x_slot = (xx * 2 + c, yy * 2 + c)

    def x_copies(role, i):
        if role == 0:
            to = turned(xx, i, nq)
            target = there(yy * nq + to, 0)
            pieces = [
                (
                    x_ref.at[:, lanes((b * nq + to) * 128, 128)],
                    xg_s.at[x_slot[0], :, pl.ds(b * 128, 128)],
                )
                for b in range(nq)
            ]
        else:
            to = turned(yy, i, nq)
            target = there(to * nq + xx, 1)
            pieces = [(x_ref.at[:, lanes(to * nq * 128, nq * 128)], xg_s.at[x_slot[1]])]
        return target, pieces

    def send_x(role, i):
        target, pieces = x_copies(role, i)

        def away():
            for src, dst in pieces:
                remote(src, dst, x_ss.at[role, i], x_rs.at[x_slot[role]], target).start()

        def at_home():
            for src, dst in pieces:
                pltpu.make_async_copy(src, dst, x_rs.at[x_slot[role]]).start()

        if i == 0:
            pl.when(c != role)(away)
            pl.when(c == role)(at_home)
        else:
            away()

    for role in range(2):
        for i in range(nq):
            send_x(role, i)

    row = lax.broadcasted_iota(jnp.int32, (BLOCK, BLOCK), 0)
    col = lax.broadcasted_iota(jnp.int32, (BLOCK, BLOCK), 1)
    left_half = lax.broadcasted_iota(jnp.int32, (64, 128), 1) < 64
    lane = lax.broadcasted_iota(jnp.int32, (BLOCK, 128), 1)
    mask0 = jnp.where(lane < 64, 1.0, 0.0).astype(BF16)
    mask1 = jnp.where(lane < 64, 0.0, 1.0).astype(BF16)
    upto = jnp.where(row >= col, 1.0, 0.0).astype(BF16)
    onward = jnp.where(row <= col, 1.0, 0.0).astype(BF16)

    def diagonal(m):
        return jnp.where(left_half, m[:64], m[64:])

    def local_states(p, _):
        at = lanes(p * 128, 128)
        gate = g_ref[:, at]
        running = nn(upto, gate)
        exclusive = running - gate.astype(F32)
        run_s[:, at] = running
        end = jnp.exp(running[BLOCK - 1 : BLOCK])
        end_s[:, at] = jnp.broadcast_to(end, (8, 128))
        query = q_ref[:, at].astype(F32) * HEAD_DIM ** (-0.5)
        key = k_ref[:, at].astype(F32)
        qf = (query * jnp.exp(running)).astype(BF16)
        kf = (key * jnp.exp(-running)).astype(BF16)
        qb = (query * jnp.exp(-exclusive)).astype(BF16)
        kb = (key * jnp.exp(exclusive)).astype(BF16)
        qf_s[:, at] = qf
        kf_s[:, at] = kf
        qb_s[:, at] = qb
        kb_s[:, at] = kb
        value = v_ref[:, at]
        cot = cot_ref[:, at]
        uh = diagonal(tn(value, kf))
        wb = diagonal(tn(cot, qb))
        raw_s[2 * p] = uh
        raw_s[2 * p + 1] = wb
        loc_s[0, 2 * p] = uh * end
        loc_s[0, 2 * p + 1] = wb * end
        loc_s[1, 2 * p] = diagonal(tn(cot, qf))
        loc_s[1, 2 * p + 1] = diagonal(tn(value, kb))
        return 0

    lax.fori_loop(0, PAIRS, local_states, 0)

    w_here.wait()
    w0.wait()
    w1 = [
        remote(
            wv_s.at[c, chip], wv_s.at[c, chip], w1_ss.at[i - 1], w1_rs.at[i - 1],
            there(chip_at(turned(pa, i, nq), pb), c),
        )
        for i in range(1, nq)
    ]
    for copy in w1:
        copy.start()

    def both(a):
        return jnp.concatenate([a * mask0, a * mask1], axis=0)

    row2 = lax.broadcasted_iota(jnp.int32, (BLOCK, 256), 0)
    col2 = lax.rem(lax.broadcasted_iota(jnp.int32, (BLOCK, 256), 1), 128)
    lower = row2 >= col2
    upper = row2 <= col2

    def own_part(p, _):
        at = lanes(p * 128, 128)
        value = v_ref[:, at]
        cot = cot_ref[:, at]
        qf, kf, qb, kb = qf_s[:, at], kf_s[:, at], qb_s[:, at], kb_s[:, at]
        value2, cot2 = both(value), both(cot)
        qf2, kf2, qb2, kb2 = both(qf), both(kf), both(qb), both(kb)
        d_score = nt(cot, value2)
        d_score_t = nt(value, cot2)
        score_t = jnp.where(upper, nt(kf, qf2), 0.0) + jnp.where(lower, nt(kb, qb2), 0.0)
        dqf_s[:, at] = nn(jnp.where(lower, d_score, 0.0).astype(BF16), kf2)
        dqb_s[:, at] = nn(jnp.where(upper, d_score, 0.0).astype(BF16), kb2)
        dkf_s[:, at] = nn(jnp.where(upper, d_score_t, 0.0).astype(BF16), qf2)
        dkb_s[:, at] = nn(jnp.where(lower, d_score_t, 0.0).astype(BF16), qb2)
        dv_s[:, at] = nn(score_t.astype(BF16), cot2)
        return 0

    def own_parts():
        lax.fori_loop(0, PAIRS, own_part, 0)

    @pl.when(z == 0)
    def _():
        recv_s[0] = jnp.zeros(recv_s.shape[1:], BF16)

    @pl.when(z == nz - 1)
    def _():
        recv_s[1] = jnp.zeros(recv_s.shape[1:], BF16)

    def chain_copy(way, j):
        return remote(
            send_s.at[way, j], recv_s.at[way, j], chain_ss.at[way, j], chain_rs.at[way, j],
            there(chip, c, lax.rem(z + 1 - 2 * way + nz, nz)),
        )

    def before(way):
        return z + way * (nz - 1 - 2 * z)

    def chain(way):
        def one(j, _):
            copy = chain_copy(way, j)

            @pl.when(before(way) > 0)
            def _():
                copy.wait_recv()

            @pl.when(before(way) < nz - 1)
            def _():
                end = end_s[0:1, lanes(lax.div(j, 2) * 128, 128)]
                state = recv_s[way, j].astype(F32) * end + loc_s[way, j]
                send_s[way, j] = state.astype(BF16)
                copy.start()

            return 0

        lax.fori_loop(0, CHUNKS, one, 0)

    first = lax.div(2 * z, nz)
    edge = jnp.minimum(z, nz - 1 - z)
    pl.when(edge >= 2)(own_parts)
    chain(first)
    pl.when(edge < 2)(own_parts)

    for copy in w1:
        copy.wait()
    w2 = []
    for i in range(1, nq):
        for j in range(nq):
            block = wv_s.at[c, chip_at(j, pb)]
            w2.append(
                remote(
                    block, block, w2_ss.at[(i - 1) * nq + j], w2_rs.at[(i - 1) * nq + j],
                    there(chip_at(pa, turned(pb, i, nq)), c),
                )
            )
    for copy in w2:
        copy.start()

    chain(1 - first)

    for copy in w2:
        copy.wait()
    w3 = remote(wv_s.at[c], wv_s.at[c], w3_ss, w3_rs, there(chip, 1 - c))
    w3.start()

    def spread(state):
        zero = jnp.zeros_like(state)
        return jnp.concatenate(
            [jnp.where(left_half, state, zero), jnp.where(left_half, zero, state)], axis=0
        ).astype(BF16)

    def finish(p, _):
        at = lanes(p * 128, 128)
        value = v_ref[:, at]
        cot = cot_ref[:, at]
        qf, kf, qb, kb = qf_s[:, at], kf_s[:, at], qb_s[:, at], kb_s[:, at]
        end = end_s[0:1, at]
        h_state = recv_s[0, 2 * p].astype(F32)
        f_state = recv_s[0, 2 * p + 1].astype(F32)
        e_state = (recv_s[1, 2 * p].astype(F32) * end).astype(BF16).astype(F32)
        r_state = (recv_s[1, 2 * p + 1].astype(F32) * end).astype(BF16).astype(F32)
        carry = jnp.sum(
            e_state * (h_state + raw_s[2 * p]) + r_state * (f_state + raw_s[2 * p + 1]),
            axis=0,
            keepdims=True,
        )
        h2, f2, e2, r2 = spread(h_state), spread(f_state), spread(e_state), spread(r_state)
        dqf = dqf_s[:, at] + nn(cot, h2)
        dqb = dqb_s[:, at] + nn(cot, r2)
        dkf = dkf_s[:, at] + nn(value, e2)
        dkb = dkb_s[:, at] + nn(value, f2)
        dvb_s[:, at] = (dv_s[:, at] + nt(kf, e2) + nt(kb, f2)).astype(BF16)
        running = run_s[:, at]
        exclusive = running - g_ref[:, at].astype(F32)
        dq = (jnp.exp(running) * dqf + jnp.exp(-exclusive) * dqb) * HEAD_DIM ** (-0.5)
        dk = jnp.exp(-running) * dkf + jnp.exp(exclusive) * dkb
        dq_ref[:, at] = dq.astype(BF16)
        dk_ref[:, at] = dk.astype(BF16)
        fwd = qf.astype(F32) * dqf - kf.astype(F32) * dkf
        bwd = kb.astype(F32) * dkb - qb.astype(F32) * dqb
        both_ways = fwd + bwd
        high = both_ways.astype(BF16)
        low = (both_ways - high.astype(F32)).astype(BF16)
        dg = nn(onward, high) + nn(onward, low) - bwd + carry
        dg_ref[:, at] = dg.astype(BF16)
        return 0

    lax.fori_loop(0, PAIRS, finish, 0)

    def send_dv(role, i):
        if role == 0:
            target = there(yy * nq + turned(xx, i, nq), 0)
        else:
            target = there(turned(yy, i, nq) * nq + xx, 1)
        src = dvb_s.at[:, pl.ds(role * HALF, HALF)]
        dst = dvg_s.at[x_slot[role]]

        def away():
            remote(src, dst, dv_ss.at[role, i], dv_rs.at[x_slot[role]], target).start()

        def at_home():
            pltpu.make_async_copy(src, dst, dv_rs.at[x_slot[role]]).start()

        if i == 0:
            pl.when(c != role)(away)
            pl.when(c == role)(at_home)
        else:
            away()

    for role in range(2):
        for i in range(nq):
            send_dv(role, i)

    w3.wait()
    group = nq * 128
    for i in range(nq):
        low_half = wv_s[0, i * nq : (i + 1) * nq].reshape(group, HALF)
        high_half = wv_s[1, i * nq : (i + 1) * nq].reshape(group, HALF)
        gi_ref[:, i * group : (i + 1) * group] = (
            nt(dvb_s[:, :HALF], low_half) + nt(dvb_s[:, HALF:], high_half)
        ).astype(BF16)

    for slot in range(2 * nq):
        remote(
            xg_s.at[slot], xg_s.at[slot], x_ss.at[0, 0], x_rs.at[slot], there(chip, 1 - c)
        ).wait_recv()
        remote(
            dvg_s.at[slot], dvg_s.at[slot], dv_ss.at[0, 0], dv_rs.at[slot], there(chip, 1 - c)
        ).wait_recv()
    tokens = 2 * nq * BLOCK
    all_dv = dvg_s[...].reshape(tokens, HALF)
    for b in range(nq):
        part = tn(xg_s[:, :, b * 128 : (b + 1) * 128].reshape(tokens, 128), all_dv)
        part_s[b] = part
        pb_s[b] = part.astype(BF16)

    s2 = [
        remote(
            pb_s.at[turned(pb, i, nq)], s2_s.at[i - 1], s2_ss.at[i - 1], s2_rs.at[i - 1],
            there(chip_at(pa, turned(pb, i, nq)), c),
        )
        for i in range(1, nq)
    ]
    for copy in s2:
        copy.start()
    total = part_s[pb]
    for i, copy in enumerate(s2):
        copy.wait()
        total = total + s2_s[i].astype(F32)
    acc_s[...] = total

    wide = nz // 4
    chunk = HALF // wide
    for j in range(nz):
        rows, columns = j // wide, j % wide
        zb_s[j] = acc_s[
            rows * 32 : (rows + 1) * 32, columns * chunk : (columns + 1) * chunk
        ].astype(BF16)

    def z_copy(i):
        to = turned(z, i, nz)
        return remote(
            zb_s.at[to], zr_s.at[i], zr_ss.at[i], zr_rs.at[i], there(chip, c, to)
        )

    def z_start(i, _):
        z_copy(i).start()
        return 0

    lax.fori_loop(1, nz, z_start, 0)

    def z_sum(i, summed):
        z_copy(i).wait()
        return summed + zr_s[i].astype(F32)

    summed = lax.fori_loop(1, nz, z_sum, zb_s[z].astype(F32))
    rb_s[...] = summed.astype(BF16)

    owner = lax.div(2 * z, nz)
    slot = c * (nz // 2) + lax.rem(z, nz // 2)

    def out_copy(i):
        return remote(
            rb_s, gr_s.at[slot], za_ss.at[i], za_rs.at[slot], there(chip, owner, turned(z, i, nz))
        )

    home = pltpu.make_async_copy(rb_s, gr_s.at[slot], za_rs.at[slot])
    pl.when(owner == c)(lambda: home.start())
    pl.when(owner != c)(lambda: out_copy(0).start())

    def out_start(i, _):
        out_copy(i).start()
        return 0

    lax.fori_loop(1, nz, out_start, 0)

    for role in range(2):
        for t in range(nz // 2):
            s = role * (nz // 2) + t
            remote(
                rb_s, gr_s.at[s], za_ss.at[0], za_rs.at[s], there(chip, 1 - c)
            ).wait_recv()
            rows, columns = t // wide, t % wide
            gw_ref[
                rows * 32 : (rows + 1) * 32,
                role * HALF + columns * chunk : role * HALF + (columns + 1) * chunk,
            ] = gr_s[s].astype(F32)

    pl.when(owner != c)(lambda: out_copy(0).wait_send())

    def out_sent(i, _):
        out_copy(i).wait_send()
        return 0

    lax.fori_loop(1, nz, out_sent, 0)

    for way in range(2):

        @pl.when(before(way) < nz - 1)
        def _():
            def sent(j, _):
                chain_copy(way, j).wait_send()
                return 0

            lax.fori_loop(0, CHUNKS, sent, 0)

    for role in range(2):
        for i in range(nq):

            def sent():
                remote(
                    xg_s.at[0], xg_s.at[0], x_ss.at[role, i], x_rs.at[0], there(chip, 1 - c)
                ).wait_send()
                remote(
                    dvg_s.at[0], dvg_s.at[0], dv_ss.at[role, i], dv_rs.at[0], there(chip, 1 - c)
                ).wait_send()

            if i == 0:
                pl.when(c != role)(sent)
            else:
                sent()


def per_device(nz, nq, inputs, queries, keys, values, log_decay, cotangent, value_weight):
    model = inputs.shape[2]
    slots = 2 * nq
    chunk = HALF // (nz // 4)
    dma = pltpu.SemaphoreType.DMA
    vm = pltpu.VMEM
    wide = jax.ShapeDtypeStruct((BLOCK, WIDTH), BF16)
    outs = pl.pallas_call(
        functools.partial(kernel, nz, nq),
        out_shape=(
            wide,
            wide,
            wide,
            jax.ShapeDtypeStruct((BLOCK, model), BF16),
            jax.ShapeDtypeStruct((64, WIDTH), F32),
        ),
        in_specs=[pl.BlockSpec(memory_space=pltpu.VMEM)] * 7,
        out_specs=[pl.BlockSpec(memory_space=pltpu.VMEM)] * 5,
        scratch_shapes=[
            vm((BLOCK, WIDTH), F32),
            vm((8, WIDTH), F32),
            *[vm((BLOCK, WIDTH), BF16)] * 4,
            vm((2, CHUNKS, 64, 128), F32),
            vm((CHUNKS, 64, 128), F32),
            vm((2, CHUNKS, 64, 128), BF16),
            vm((2, CHUNKS, 64, 128), BF16),
            *[vm((BLOCK, WIDTH), F32)] * 5,
            vm((BLOCK, WIDTH), BF16),
            vm((2, nq * nq, 128, HALF), BF16),
            vm((slots, BLOCK, nq * 128), BF16),
            vm((slots, BLOCK, HALF), BF16),
            vm((nq, 128, HALF), F32),
            vm((nq, 128, HALF), BF16),
            vm((nq - 1, 128, HALF), BF16),
            vm((128, HALF), F32),
            vm((nz, 32, chunk), BF16),
            vm((nz, 32, chunk), BF16),
            vm((32, chunk), BF16),
            vm((nz, 32, chunk), BF16),
            dma((2, CHUNKS)),
            dma((2, CHUNKS)),
            dma, dma, dma,
            dma((nq - 1,)), dma((nq - 1,)),
            dma(((nq - 1) * nq,)), dma(((nq - 1) * nq,)),
            dma, dma,
            dma((2, nq)), dma((slots,)),
            dma((2, nq)), dma((slots,)),
            dma((nq - 1,)), dma((nq - 1,)),
            dma((nz,)), dma((nz,)),
            dma((nz,)), dma((nz,)),
        ],
        compiler_params=pltpu.CompilerParams(
            collective_id=0, has_side_effects=True, vmem_limit_bytes=60 * 1024 * 1024
        ),
    )(
        queries[0], keys[0], values[0], log_decay[0], cotangent[0], inputs[0], value_weight
    )
    dq, dk, dg, gi, gw = outs
    return dq[None], dk[None], dg[None], gi[None], gw


def solution(mesh):
    nz = mesh.shape["sp"]
    nq = 4 if mesh.shape["dp"] == 32 else 2
    tokens = P("dp", "sp", None)
    return jax.shard_map(
        functools.partial(per_device, nz, nq),
        mesh=mesh,
        in_specs=(tokens,) * 6 + (P("dp", None),),
        out_specs=(tokens,) * 4 + (P("dp", None),),
        check_vma=False,
    )
```

time: 524 us -> 110 us (0.21)
  the two profiles are of different devices: /device:TPU:32 before, /device:TPU:1 now
where the time goes in v1:
time: 110 us
  Pallas kernels  104 us (95%)
  local copies, waits for them, and re-layouts  4.94 us (4%)
    pallas_call x1, Pallas kernels, per_device(): pl.pallas_call(functools.partial(kernel, nz, nq), out_shape=(wide, wide,...  104 us
    unnamed x13, local copies, waits for them, and re-layouts  4.94 us

profile of v1, /device:TPU:1, one launch (start us, length us, event | category | flops | bytes accessed | tf_op | source)
XLA Modules:
  0.0 110.0 jit_solution(13403698058519559558)
XLA Ops:
  0.6 104.4 %shard_map.110 = (bf16[128,1024]{1,0:T(8,128)(2,1)}, bf16[128,1024]{1,0:T(8,128)(2,1)}, bf16[128,1024]{1,0:T(8,128)(2,1)}, bf16[128,2048]{1,0:T(8,128)(2,1)}, f32[64,1024]{1,0:T(8,128)}) custom-call(bf16[128,1024]{1,0:T(8,128)(2,1)} %bitcast.12, bf16[128,1024]{1,0:T(8,128)(2,1)} %bitcast.13, bf16[128,1024]{1,0:T(8,128)(2,1)} %bitcast.14, ...), custom_call_target="tpu_custom_call" | custom-call | tf_op jit(solution)/shard_map/pallas_call | solution.py:490
  105.0 0.0 copy-start.3
  105.0 0.0 copy-start.2
  105.0 1.7 %copy.17 = bf16[1,128,1024]{2,1,0:T(8,128)(2,1)} copy(bf16[1,128,1024]{2,1,0:T(8,128)(2,1)} %bitcast.19) | data formatting | bytes 524288
  106.8 0.0 copy-done.3
  106.8 0.0 copy-start
  106.8 0.7 copy.18
  107.5 0.0 copy-done.2
  107.5 0.7 copy.19
  108.2 0.0 copy-done
  108.2 0.0 copy-start.1
  108.2 0.8 copy.20
  109.0 0.3 copy-done.1
  109.3 0.7 copy.21
Async XLA Ops:
  105.0 1.7 %copy-start.3 = (bf16[128,1024]{1,0:T(8,128)(2,1)S(1)}, bf16[128,1024]{1,0:T(8,128)(2,1)}, u32[]{:S(2)}) copy-start(bf16[128,1024]{1,0:T(8,128)(2,1)} %get-tuple-element.11) | copy-start | bytes 786436
  105.0 2.4 %copy-start.2 = (bf16[128,1024]{1,0:T(8,128)(2,1)S(1)}, bf16[128,1024]{1,0:T(8,128)(2,1)}, u32[]{:S(2)}) copy-start(bf16[128,1024]{1,0:T(8,128)(2,1)} %get-tuple-element.12) | copy-start | bytes 786436
  106.8 1.4 %copy-start = (bf16[128,2048]{1,0:T(8,128)(2,1)S(1)}, bf16[128,2048]{1,0:T(8,128)(2,1)}, u32[]{:S(2)}) copy-start(bf16[128,2048]{1,0:T(8,128)(2,1)} %get-tuple-element.13) | copy-start | bytes 1572868
  108.2 1.1 copy-start.1

commit v2 on v1

v2 whole, which is shorter than its diff:
```python
import functools

import jax
import jax.numpy as jnp
from jax import lax
from jax.experimental import pallas as pl
from jax.experimental.pallas import tpu as pltpu
from jax.sharding import PartitionSpec as P

MESH = pl.DeviceIdType.MESH
F32 = jnp.float32
BF16 = jnp.bfloat16
BLOCK = 128
WIDTH = 1024
HALF = WIDTH // 2
PAIRS = WIDTH // 128
CHUNKS = 2 * PAIRS
HEAD_DIM = 64


def nn(a, b):
    return lax.dot_general(a, b, (((1,), (0,)), ((), ())), preferred_element_type=F32)


def nt(a, b):
    return lax.dot_general(a, b, (((1,), (1,)), ((), ())), preferred_element_type=F32)


def tn(a, b):
    return lax.dot_general(a, b, (((0,), (0,)), ((), ())), preferred_element_type=F32)


def lanes(start, size):
    return pl.ds(pl.multiple_of(start, 128), size)


def kernel(
    nz, nq,
    q_ref, k_ref, v_ref, g_ref, cot_ref, x_ref, w_ref,
    dq_ref, dk_ref, dg_ref, gi_ref, gw_ref,
    run_s, end_s, qf_s, kf_s, qb_s, kb_s, loc_s, raw_s, send_s, recv_s,
    dqf_s, dqb_s, dkf_s, dkb_s, dv_s, dvb_s,
    wv_s, xg_s, xgt_s, dvg_s, part_s, pb_s, s2_s, zb_s, zr_s, rb_s, gr_s,
    chain_ss, chain_rs, fw_ss, fw_rs, loc_ss, loc_rs,
    w0_ss, w0_rs, w_loc, w1_ss, w1_rs, w2_ss, w2_rs, w3_ss, w3_rs,
    x_ss, x_rs, dv_ss, dv_rs, s2_ss, s2_rs, zr_ss, zr_rs, za_ss, za_rs,
):
    z = lax.axis_index("sp")
    d = lax.axis_index("dp")
    c = lax.rem(d, 2)
    chip = lax.div(d, 2)
    xx = lax.rem(chip, nq)
    yy = lax.div(chip, nq)
    pa = xx * (1 - c) + yy * c
    pb = yy * (1 - c) + xx * c

    def chip_at(a, b):
        return (b * nq + a) * (1 - c) + (a * nq + b) * c

    def there(chip_id, core, at_z=None):
        return {"sp": z if at_z is None else at_z, "dp": chip_id * 2 + core}

    def turned(at, i, n):
        return lax.rem(at + i, n)

    barrier = pltpu.get_barrier_semaphore()
    greeted = 0
    for i in range(1, nq):
        for core in range(2):
            for other in (yy * nq + turned(xx, i, nq), turned(yy, i, nq) * nq + xx):
                pl.semaphore_signal(barrier, inc=1, device_id=there(other, core), device_id_type=MESH)
                greeted += 1
    pl.semaphore_signal(barrier, inc=1, device_id=there(chip, 1 - c), device_id_type=MESH)
    for step in (1, nz - 1):
        pl.semaphore_signal(
            barrier, inc=1, device_id=there(chip, c, turned(z, step, nz)), device_id_type=MESH
        )
    def remote(src, dst, ss, rs, device):
        return pltpu.make_async_remote_copy(
            src_ref=src, dst_ref=dst, send_sem=ss, recv_sem=rs, device_id=device, device_id_type=MESH
        )

    row = lax.broadcasted_iota(jnp.int32, (BLOCK, BLOCK), 0)
    col = lax.broadcasted_iota(jnp.int32, (BLOCK, BLOCK), 1)
    left_half = lax.broadcasted_iota(jnp.int32, (64, 128), 1) < 64
    lane = lax.broadcasted_iota(jnp.int32, (BLOCK, 128), 1)
    mask0 = jnp.where(lane < 64, 1.0, 0.0).astype(BF16)
    mask1 = jnp.where(lane < 64, 0.0, 1.0).astype(BF16)
    upto = jnp.where(row >= col, 1.0, 0.0).astype(BF16)
    onward = jnp.where(row <= col, 1.0, 0.0).astype(BF16)

    def diagonal(m):
        return jnp.where(left_half, m[:64], m[64:])

    def local_states(p, _):
        at = lanes(p * 128, 128)
        gate = g_ref[:, at]
        running = nn(upto, gate)
        exclusive = running - gate.astype(F32)
        run_s[:, at] = running
        end = jnp.exp(running[BLOCK - 1 : BLOCK])
        end_s[1, :, at] = jnp.broadcast_to(end, (8, 128))
        query = q_ref[:, at].astype(F32) * HEAD_DIM ** (-0.5)
        key = k_ref[:, at].astype(F32)
        qf = (query * jnp.exp(running)).astype(BF16)
        kf = (key * jnp.exp(-running)).astype(BF16)
        qb = (query * jnp.exp(-exclusive)).astype(BF16)
        kb = (key * jnp.exp(exclusive)).astype(BF16)
        qf_s[:, at] = qf
        kf_s[:, at] = kf
        qb_s[:, at] = qb
        kb_s[:, at] = kb
        value = v_ref[:, at]
        cot = cot_ref[:, at]
        uh = diagonal(tn(value, kf))
        wb = diagonal(tn(cot, qb))
        raw_s[2 * p] = uh
        raw_s[2 * p + 1] = wb
        loc_s[1, p, 0, 0] = (uh * end).astype(BF16)
        loc_s[1, p, 0, 1] = (wb * end).astype(BF16)
        loc_s[1, p, 1, 0] = diagonal(tn(cot, qf)).astype(BF16)
        loc_s[1, p, 1, 1] = diagonal(tn(value, kb)).astype(BF16)
        return 0

    lax.fori_loop(0, PAIRS, local_states, 0)

    pl.semaphore_wait(barrier, greeted + 3)

    def state_copies():
        return (
            remote(loc_s.at[1], loc_s.at[0], loc_ss.at[0], loc_rs.at[0], there(chip, 1 - c)),
            remote(end_s.at[1], end_s.at[0], loc_ss.at[1], loc_rs.at[1], there(chip, 1 - c)),
        )

    @pl.when(c == 0)
    def _():
        for copy in state_copies():
            copy.start()

    w_here = pltpu.make_async_copy(
        w_ref.at[:, lanes(c * HALF, HALF)],
        wv_s.at[c, chip, pl.ds(pl.multiple_of(c * 64, 64), 64), :],
        w_loc,
    )
    w_here.start()
    w0 = remote(
        w_ref.at[:, lanes((1 - c) * HALF, HALF)],
        wv_s.at[1 - c, chip, pl.ds(pl.multiple_of(c * 64, 64), 64), :],
        w0_ss, w0_rs, there(chip, 1 - c),
    )
    w0.start()

    x_slot = (xx * 2 + c, yy * 2 + c)

    def x_copies(role, i):
        if role == 0:
            to = turned(xx, i, nq)
            target = there(yy * nq + to, 0)
            pieces = [
                (
                    x_ref.at[:, lanes((b * nq + to) * 128, 128)],
                    xg_s.at[x_slot[0], :, pl.ds(b * 128, 128)],
                )
                for b in range(nq)
            ]
        else:
            to = turned(yy, i, nq)
            target = there(to * nq + xx, 1)
            pieces = [(x_ref.at[:, lanes(to * nq * 128, nq * 128)], xg_s.at[x_slot[1]])]
        return target, pieces

    def send_x(role, i):
        target, pieces = x_copies(role, i)

        def away():
            for src, dst in pieces:
                remote(src, dst, x_ss.at[role, i], x_rs.at[x_slot[role]], target).start()

        def at_home():
            for src, dst in pieces:
                pltpu.make_async_copy(src, dst, x_rs.at[x_slot[role]]).start()

        if i == 0:
            pl.when(c != role)(away)
            pl.when(c == role)(at_home)
        else:
            away()

    for role in range(2):
        for i in range(nq):
            send_x(role, i)

    w_here.wait()
    w0.wait()
    w1 = [
        remote(
            wv_s.at[c, chip], wv_s.at[c, chip], w1_ss.at[i - 1], w1_rs.at[i - 1],
            there(chip_at(turned(pa, i, nq), pb), c),
        )
        for i in range(1, nq)
    ]
    for copy in w1:
        copy.start()

    def both(a):
        return jnp.concatenate([a * mask0, a * mask1], axis=0)

    row2 = lax.broadcasted_iota(jnp.int32, (BLOCK, 256), 0)
    col2 = lax.rem(lax.broadcasted_iota(jnp.int32, (BLOCK, 256), 1), 128)
    lower = row2 >= col2
    upper = row2 <= col2

    def own_part(p, _):
        at = lanes(p * 128, 128)
        value = v_ref[:, at]
        cot = cot_ref[:, at]
        qf, kf, qb, kb = qf_s[:, at], kf_s[:, at], qb_s[:, at], kb_s[:, at]
        value2, cot2 = both(value), both(cot)
        qf2, kf2, qb2, kb2 = both(qf), both(kf), both(qb), both(kb)
        d_score = nt(cot, value2)
        d_score_t = nt(value, cot2)
        score_t = jnp.where(upper, nt(kf, qf2), 0.0) + jnp.where(lower, nt(kb, qb2), 0.0)
        dqf_s[:, at] = nn(jnp.where(lower, d_score, 0.0).astype(BF16), kf2)
        dqb_s[:, at] = nn(jnp.where(upper, d_score, 0.0).astype(BF16), kb2)
        dkf_s[:, at] = nn(jnp.where(upper, d_score_t, 0.0).astype(BF16), qf2)
        dkb_s[:, at] = nn(jnp.where(lower, d_score_t, 0.0).astype(BF16), qb2)
        dv_s[:, at] = nn(score_t.astype(BF16), cot2)
        return 0

    def prepare():
        lax.fori_loop(0, PAIRS, own_part, 0)
        for slot in range(2 * nq):
            remote(
                xg_s.at[slot], xg_s.at[slot], x_ss.at[0, 0], x_rs.at[slot], there(chip, 1 - c)
            ).wait_recv()
            for b in range(nq):
                xgt_s[b, :, slot * BLOCK : (slot + 1) * BLOCK] = xg_s[
                    slot, :, b * 128 : (b + 1) * 128
                ].T

    def before(way):
        return z + way * (nz - 1 - 2 * z)

    for way in range(2):

        @pl.when(before(way) == 0)
        def _():
            recv_s[:, way] = jnp.zeros((2, *recv_s.shape[2:]), BF16)

    def chain_copy(s, way, j):
        return remote(
            send_s.at[s, way, j], recv_s.at[s, way, j],
            chain_ss.at[s, way, j], chain_rs.at[s, way, j],
            there(chip, c, lax.rem(z + 1 - 2 * way + nz, nz)),
        )

    def forward_copy(way, j):
        return remote(
            recv_s.at[0, way, j], recv_s.at[1, way, j],
            fw_ss.at[way, j], fw_rs.at[way, j], there(chip, 1 - c),
        )

    first = lax.div(2 * z, nz)
    edge = jnp.minimum(z, nz - 1 - z)
    steps = 2 * CHUNKS
    lead = 6
    lag = jnp.where(edge == nz // 2 - 1, 12, steps)

    def chain_step(t, _):
        turn = t - lag
        second = jnp.where(t < lag, 0, jnp.where(t < 2 * steps - lag, lax.rem(turn, 2), 1))
        index = jnp.where(
            t < lag,
            t,
            jnp.where(
                t < 2 * steps - lag,
                lax.div(turn, 2) + lag * (1 - lax.rem(turn, 2)),
                t - steps,
            ),
        )
        way = first + second - 2 * first * second
        theirs = jnp.where((index >= lead) & (index < lead + CHUNKS), 1, 0)
        s = 1 - theirs
        j = index - jnp.where(index < lead, 0, jnp.where(theirs == 1, lead, CHUNKS))
        copy = chain_copy(s, way, j)

        @pl.when(t == lead)
        def _():
            for taken in state_copies():
                taken.wait_recv()

        @pl.when(before(way) > 0)
        def _():
            copy.wait_recv()

            @pl.when(theirs == 1)
            def _():
                forward_copy(way, j).start()

        @pl.when(before(way) < nz - 1)
        def _():
            pair = lax.div(j, 2)
            end = end_s[s, 0:1, lanes(pair * 128, 128)]
            own = loc_s[s, pair, way, lax.rem(j, 2)].astype(F32)
            state = recv_s[s, way, j].astype(F32) * end + own
            send_s[s, way, j] = state.astype(BF16)
            copy.start()

        return 0

    early = edge >= nz // 4
    pl.when((c == 0) | early)(prepare)

    def chain(begin):
        @pl.when(c == 1)
        def _():
            lax.fori_loop(begin, begin + steps, chain_step, 0)

    chain(0)
    pl.when((c == 1) & (edge < nz // 4))(prepare)

    for copy in w1:
        copy.wait()
    w2 = []
    for i in range(1, nq):
        for j in range(nq):
            block = wv_s.at[c, chip_at(j, pb)]
            w2.append(
                remote(
                    block, block, w2_ss.at[(i - 1) * nq + j], w2_rs.at[(i - 1) * nq + j],
                    there(chip_at(pa, turned(pb, i, nq)), c),
                )
            )
    for copy in w2:
        copy.start()

    chain(steps)

    for copy in w2:
        copy.wait()
    w3 = remote(wv_s.at[c], wv_s.at[c], w3_ss, w3_rs, there(chip, 1 - c))
    w3.start()

    for way in range(2):

        @pl.when((c == 0) & (before(way) > 0))
        def _():
            def back(j, _):
                forward_copy(way, j).wait_recv()
                return 0

            lax.fori_loop(0, CHUNKS, back, 0)

    def spread(state):
        zero = jnp.zeros_like(state)
        return jnp.concatenate(
            [jnp.where(left_half, state, zero), jnp.where(left_half, zero, state)], axis=0
        ).astype(BF16)

    def value_part(i, _):
        p = lax.rem(i, 2) * (PAIRS // 2) + lax.div(i, 2)
        at = lanes(p * 128, 128)
        e2 = spread(recv_s[1, 1, 2 * p].astype(F32) * end_s[1, 0:1, at])
        f2 = spread(recv_s[1, 0, 2 * p + 1].astype(F32))
        dvb_s[:, at] = (dv_s[:, at] + nt(kf_s[:, at], e2) + nt(kb_s[:, at], f2)).astype(BF16)
        return 0

    def send_dv(h, role, i):
        if role == 0:
            target = there(yy * nq + turned(xx, i, nq), 0)
        else:
            target = there(turned(yy, i, nq) * nq + xx, 1)
        src = dvb_s.at[:, pl.ds(role * HALF + h * 256, 256)]
        dst = dvg_s.at[h, x_slot[role]]

        def away():
            remote(
                src, dst, dv_ss.at[h, role, i], dv_rs.at[h, x_slot[role]], target
            ).start()

        def at_home():
            pltpu.make_async_copy(src, dst, dv_rs.at[h, x_slot[role]]).start()

        if i == 0:
            pl.when(c != role)(away)
            pl.when(c == role)(at_home)
        else:
            away()

    for h in range(2):
        lax.fori_loop(h * (PAIRS // 2), (h + 1) * (PAIRS // 2), value_part, 0)
        for i in (2, 1, 3, 0) if nq == 4 else (1, 0):
            for role in range(2):
                send_dv(h, role, i)

    def finish(p, _):
        at = lanes(p * 128, 128)
        value = v_ref[:, at]
        cot = cot_ref[:, at]
        qf, kf, qb, kb = qf_s[:, at], kf_s[:, at], qb_s[:, at], kb_s[:, at]
        end = end_s[1, 0:1, at]
        h_state = recv_s[1, 0, 2 * p].astype(F32)
        f_state = recv_s[1, 0, 2 * p + 1].astype(F32)
        e_state = (recv_s[1, 1, 2 * p].astype(F32) * end).astype(BF16).astype(F32)
        r_state = (recv_s[1, 1, 2 * p + 1].astype(F32) * end).astype(BF16).astype(F32)
        carry = jnp.sum(
            e_state * (h_state + raw_s[2 * p]) + r_state * (f_state + raw_s[2 * p + 1]),
            axis=0,
            keepdims=True,
        )
        h2, f2, e2, r2 = spread(h_state), spread(f_state), spread(e_state), spread(r_state)
        dqf = dqf_s[:, at] + nn(cot, h2)
        dqb = dqb_s[:, at] + nn(cot, r2)
        dkf = dkf_s[:, at] + nn(value, e2)
        dkb = dkb_s[:, at] + nn(value, f2)
        running = run_s[:, at]
        exclusive = running - g_ref[:, at].astype(F32)
        dq = (jnp.exp(running) * dqf + jnp.exp(-exclusive) * dqb) * HEAD_DIM ** (-0.5)
        dk = jnp.exp(-running) * dkf + jnp.exp(exclusive) * dkb
        dq_ref[:, at] = dq.astype(BF16)
        dk_ref[:, at] = dk.astype(BF16)
        fwd = qf.astype(F32) * dqf - kf.astype(F32) * dkf
        bwd = kb.astype(F32) * dkb - qb.astype(F32) * dqb
        both_ways = fwd + bwd
        high = both_ways.astype(BF16)
        low = (both_ways - high.astype(F32)).astype(BF16)
        dg = nn(onward, high) + nn(onward, low) - bwd + carry
        dg_ref[:, at] = dg.astype(BF16)
        return 0

    lax.fori_loop(0, PAIRS, finish, 0)

    w3.wait()
    group = nq * 128
    for i in range(nq):
        low_half = wv_s[0, i * nq : (i + 1) * nq].reshape(group, HALF)
        high_half = wv_s[1, i * nq : (i + 1) * nq].reshape(group, HALF)
        gi_ref[:, i * group : (i + 1) * group] = (
            nt(dvb_s[:, :HALF], low_half) + nt(dvb_s[:, HALF:], high_half)
        ).astype(BF16)

    tokens = 2 * nq * BLOCK

    def s2_copies(h):
        return [
            remote(
                pb_s.at[h, turned(pb, i, nq)], s2_s.at[h, i - 1],
                s2_ss.at[h, i - 1], s2_rs.at[h, i - 1],
                there(chip_at(pa, turned(pb, i, nq)), c),
            )
            for i in range(1, nq)
        ]

    for h in range(2):
        for slot in range(2 * nq):
            remote(
                dvg_s.at[h, slot], dvg_s.at[h, slot], dv_ss.at[0, 0, 0], dv_rs.at[h, slot],
                there(chip, 1 - c),
            ).wait_recv()
        gathered = dvg_s[h].reshape(tokens, 256)
        for b in range(nq):
            part = nn(xgt_s[b], gathered)
            part_s[h, b] = part
            pb_s[h, b] = part.astype(BF16)
        for copy in s2_copies(h):
            copy.start()

    wide = 4 if nz == 16 else 2
    stack = nz // wide
    height = 128 // stack
    chunk = HALF // wide

    def z_copy(to):
        return remote(zb_s.at[to], zr_s.at[z], zr_ss.at[to], zr_rs.at[z], there(chip, c, to))

    for h in range(2):
        total = part_s[h, pb]
        for i, copy in enumerate(s2_copies(h)):
            copy.wait()
            total = total + s2_s[h, i].astype(F32)
        per = wide // 2
        for r in range(stack):
            for l in range(per):
                zb_s[r * wide + h * per + l] = total[
                    r * height : (r + 1) * height, l * chunk : (l + 1) * chunk
                ].astype(BF16)
        for r in (2, 1, 3, 0) if stack == 4 else (1, 0):
            group_at = lax.rem(lax.div(z, wide) + r, stack)
            for l in range(per):
                to = group_at * wide + h * per + l
                pl.when(to != z)(lambda: z_copy(to).start())

    zr_s[z] = zb_s[z]

    def z_wait(source, _):
        @pl.when(source != z)
        def _():
            remote(
                zb_s.at[source], zr_s.at[source], zr_ss.at[source], zr_rs.at[source],
                there(chip, c, source),
            ).wait()

        return 0

    lax.fori_loop(0, nz, z_wait, 0)
    rb_s[...] = jnp.sum(zr_s[...].astype(F32), axis=0).astype(BF16)

    owner = lax.div(2 * z, nz)
    slot = c * (nz // 2) + lax.rem(z, nz // 2)

    def out_copy(i):
        return remote(
            rb_s, gr_s.at[slot], za_ss.at[i], za_rs.at[slot], there(chip, owner, turned(z, i, nz))
        )

    home = pltpu.make_async_copy(rb_s, gr_s.at[slot], za_rs.at[slot])
    for near in range(nz // 2):
        out_copy(nz // 2 - near).start()
        if near > 0:
            out_copy(nz // 2 + near).start()
    pl.when(owner == c)(lambda: home.start())
    pl.when(owner != c)(lambda: out_copy(0).start())

    for role in range(2):
        for t in range(nz // 2):
            s = role * (nz // 2) + t
            remote(
                rb_s, gr_s.at[s], za_ss.at[0], za_rs.at[s], there(chip, 1 - c)
            ).wait_recv()
            rows, columns = t // wide, t % wide
            gw_ref[
                rows * height : (rows + 1) * height,
                role * HALF + columns * chunk : role * HALF + (columns + 1) * chunk,
            ] = gr_s[s].astype(F32)

    pl.when(owner != c)(lambda: out_copy(0).wait_send())

    def out_sent(i, _):
        out_copy(i).wait_send()
        return 0

    lax.fori_loop(1, nz, out_sent, 0)

    @pl.when(c == 0)
    def _():
        for copy in state_copies():
            copy.wait_send()

    for way in range(2):

        @pl.when((c == 1) & (before(way) < nz - 1))
        def _():
            def sent(j, _):
                for s in range(2):
                    chain_copy(s, way, j).wait_send()
                return 0

            lax.fori_loop(0, CHUNKS, sent, 0)

        @pl.when((c == 1) & (before(way) > 0))
        def _():
            def sent(j, _):
                forward_copy(way, j).wait_send()
                return 0

            lax.fori_loop(0, CHUNKS, sent, 0)

    for role in range(2):
        for i in range(nq):

            def sent():
                remote(
                    xg_s.at[0], xg_s.at[0], x_ss.at[role, i], x_rs.at[0], there(chip, 1 - c)
                ).wait_send()
                for h in range(2):
                    remote(
                        dvg_s.at[h, 0], dvg_s.at[h, 0], dv_ss.at[h, role, i], dv_rs.at[h, 0],
                        there(chip, 1 - c),
                    ).wait_send()

            if i == 0:
                pl.when(c != role)(sent)
            else:
                sent()


def store(*refs):
    count = len(refs) // 3
    sources, targets, sems = refs[:count], refs[count : 2 * count], refs[2 * count :]
    copies = [pltpu.make_async_copy(*each) for each in zip(sources, targets, sems)]
    for copy in copies:
        copy.start()
    for copy in copies:
        copy.wait()


def per_device(nz, nq, inputs, queries, keys, values, log_decay, cotangent, value_weight):
    model = inputs.shape[2]
    slots = 2 * nq
    wide = 4 if nz == 16 else 2
    chunk = (128 * wide // nz, HALF // wide)
    dma = pltpu.SemaphoreType.DMA
    vm = pltpu.VMEM
    shapes = [((BLOCK, WIDTH), BF16)] * 3 + [((BLOCK, model), BF16), ((64, WIDTH), F32)]
    in_vmem = pl.BlockSpec(memory_space=pltpu.VMEM)
    anywhere = pl.BlockSpec(memory_space=pl.ANY)
    outs = pl.pallas_call(
        functools.partial(kernel, nz, nq),
        out_shape=tuple(vm(*shape) for shape in shapes),
        in_specs=[in_vmem] * 5 + [anywhere] * 2,
        out_specs=[in_vmem] * 5,
        scratch_shapes=[
            vm((BLOCK, WIDTH), F32),
            vm((2, 8, WIDTH), F32),
            *[vm((BLOCK, WIDTH), BF16)] * 4,
            vm((2, PAIRS, 2, 2, 64, 128), BF16),
            vm((CHUNKS, 64, 128), F32),
            vm((2, 2, CHUNKS, 64, 128), BF16),
            vm((2, 2, CHUNKS, 64, 128), BF16),
            *[vm((BLOCK, WIDTH), F32)] * 5,
            vm((BLOCK, WIDTH), BF16),
            vm((2, nq * nq, 128, HALF), BF16),
            vm((slots, BLOCK, nq * 128), BF16),
            vm((nq, 128, slots * BLOCK), BF16),
            vm((2, slots, BLOCK, 256), BF16),
            vm((2, nq, 128, 256), F32),
            vm((2, nq, 128, 256), BF16),
            vm((2, nq - 1, 128, 256), BF16),
            vm((nz, *chunk), BF16),
            vm((nz, *chunk), BF16),
            vm(chunk, BF16),
            vm((nz, *chunk), BF16),
            dma((2, 2, CHUNKS)), dma((2, 2, CHUNKS)),
            dma((2, CHUNKS)), dma((2, CHUNKS)),
            dma((2,)), dma((2,)),
            dma, dma, dma,
            dma((nq - 1,)), dma((nq - 1,)),
            dma(((nq - 1) * nq,)), dma(((nq - 1) * nq,)),
            dma, dma,
            dma((2, nq)), dma((slots,)),
            dma((2, 2, nq)), dma((2, slots)),
            dma((2, nq - 1)), dma((2, nq - 1)),
            dma((nz,)), dma((nz,)),
            dma((nz,)), dma((nz,)),
        ],
        compiler_params=pltpu.CompilerParams(
            collective_id=0, has_side_effects=True, vmem_limit_bytes=65_300_000
        ),
    )(
        queries[0], keys[0], values[0], log_decay[0], cotangent[0], inputs[0], value_weight
    )
    dq, dk, dg, gi, gw = pl.pallas_call(
        store,
        out_shape=tuple(jax.ShapeDtypeStruct(*shape) for shape in shapes),
        in_specs=[anywhere] * 5,
        out_specs=[anywhere] * 5,
        scratch_shapes=[dma] * 5,
        compiler_params=pltpu.CompilerParams(vmem_limit_bytes=1024 * 1024),
    )(*outs)
    return dq[None], dk[None], dg[None], gi[None], gw


def solution(mesh):
    nz = mesh.shape["sp"]
    nq = 4 if mesh.shape["dp"] == 32 else 2
    tokens = P("dp", "sp", None)
    return jax.shard_map(
        functools.partial(per_device, nz, nq),
        mesh=mesh,
        in_specs=(tokens,) * 6 + (P("dp", None),),
        out_specs=(tokens,) * 4 + (P("dp", None),),
        check_vma=False,
    )
```

time: 110 us -> 88.8 us (0.81)
  Pallas kernels: 104 us -> 88 us
  local copies, waits for them, and re-layouts: 4.94 us -> 0 us
    pallas_call x1 -> x2, Pallas kernels: 104 us -> 88 us  [the longest x1 86.8 us: per_device(): pl.pallas_call(functools.partial(kernel, nz, nq), out_shape=tuple((vm(*sh...]
    unnamed x13 -> x0, local copies, waits for them, and re-layouts: 4.94 us -> none
where the time goes in v2:
time: 88.8 us; the launch traced here: 88.7 us
  Pallas kernels  88 us (99%)
    pallas_call x1, Pallas kernels, per_device(): pl.pallas_call(functools.partial(kernel, nz, nq), out_shape=tuple((vm(*sh...  86.8 us

profile of v2, /device:TPU:1, one launch (start us, length us, event | category | flops | bytes accessed | tf_op | source)
XLA Modules:
  0.0 88.7 jit_solution(967824151438066739)
XLA Ops:
  0.6 86.8 %shard_map.110 = (bf16[128,1024]{1,0:T(8,128)(2,1)S(1)}, bf16[128,1024]{1,0:T(8,128)(2,1)S(1)}, bf16[128,1024]{1,0:T(8,128)(2,1)S(1)}, bf16[128,2048]{1,0:T(8,128)(2,1)S(1)}, f32[64,1024]{1,0:T(8,128)S(1)}) custom-call(bf16[128,1024]{1,0:T(8,128)(2,1)} %bitcast.11, bf16[128,1024]{1,0:T(8,128)(2,1)} %bitcast.12, bf16[128,1024]{1,0:T(8,128)(2,1)} %bitcast.13, ...), custom_call_target="tpu_custom_call" | custom-call | tf_op jit(solution)/shard_map/pallas_call | solution.py:607
  87.5 1.2 %shard_map.111 = (bf16[128,1024]{1,0:T(8,128)(2,1)}, bf16[128,1024]{1,0:T(8,128)(2,1)}, bf16[128,1024]{1,0:T(8,128)(2,1)}, bf16[128,2048]{1,0:T(8,128)(2,1)}, f32[64,1024]{1,0:T(8,128)}) custom-call(bf16[128,1024]{1,0:T(8,128)(2,1)S(1)} %get-tuple-element.15.refs_0_, bf16[128,1024]{1,0:T(8,128)(2,1)S(1)} %get-tuple-element.16.refs_1_, ...), custom_call_target="tpu_custom_call" | custom-call | tf_op jit(solution)/shard_map/pallas_call | solution.py:652

commit v3 on v2

v3 whole, which is shorter than its diff:
```python
import functools

import jax
import jax.numpy as jnp
from jax import lax
from jax.experimental import pallas as pl
from jax.experimental.pallas import tpu as pltpu
from jax.sharding import PartitionSpec as P

MESH = pl.DeviceIdType.MESH
F32 = jnp.float32
BF16 = jnp.bfloat16
BLOCK = 128
WIDTH = 1024
HALF = WIDTH // 2
PAIRS = WIDTH // 128
CHUNKS = 2 * PAIRS
HEAD_DIM = 64
UNROLL = 2


def nn(a, b):
    return lax.dot_general(a, b, (((1,), (0,)), ((), ())), preferred_element_type=F32)


def nt(a, b):
    return lax.dot_general(a, b, (((1,), (1,)), ((), ())), preferred_element_type=F32)


def tn(a, b):
    return lax.dot_general(a, b, (((0,), (0,)), ((), ())), preferred_element_type=F32)


def lanes(start, size):
    return pl.ds(pl.multiple_of(start, 128), size)


def kernel(
    nz, nq,
    q_in, k_in, v_in, g_in, cot_in, x_ref, w_ref,
    dq_out, dk_out, dg_out, gi_out, gr_s,
    q_ref, k_ref, v_ref, g_ref, cot_ref, dq_ref, dk_ref, dg_ref, gi_ref,
    run_s, end_s, qf_s, kf_s, qb_s, kb_s, loc_s, raw_s,
    fol_s, fend_s, in_s, out_s, state_s,
    dqf_s, dqb_s, dkf_s, dkb_s, dv_s, dvb_s,
    wv_s, xg_s, xgt_s, dvg_s, part_s, pb_s, s2_s, zb_s, zr_s, rb_s,
    in_sem, out_sem, chain_ss, chain_rs, hand_ss, hand_rs, fw_ss, fw_rs,
    loc_ss, loc_rs, fol_ss, fol_rs, fend_ss, fend_rs,
    w0_ss, w0_rs, w_loc, w1_ss, w1_rs, w2_ss, w2_rs, w3_ss, w3_rs,
    x_ss, x_rs, dv_ss, dv_rs, s2_ss, s2_rs, zr_ss, zr_rs, za_ss, za_rs,
):
    z = lax.axis_index("sp")
    d = lax.axis_index("dp")
    c = lax.rem(d, 2)
    chip = lax.div(d, 2)
    xx = lax.rem(chip, nq)
    yy = lax.div(chip, nq)
    pa = xx * (1 - c) + yy * c
    pb = yy * (1 - c) + xx * c

    def chip_at(a, b):
        return (b * nq + a) * (1 - c) + (a * nq + b) * c

    def there(chip_id, core, at_z=None):
        return {"sp": z if at_z is None else at_z, "dp": chip_id * 2 + core}

    def turned(at, i, n):
        return lax.rem(at + i, n)

    barrier = pltpu.get_barrier_semaphore()
    greeted = 0
    for i in range(1, nq):
        for core in range(2):
            for other in (yy * nq + turned(xx, i, nq), turned(yy, i, nq) * nq + xx):
                pl.semaphore_signal(barrier, inc=1, device_id=there(other, core), device_id_type=MESH)
                greeted += 1
    pl.semaphore_signal(barrier, inc=1, device_id=there(chip, 1 - c), device_id_type=MESH)
    mate = z + 1 - 2 * lax.rem(z, 2)
    for at_z, core in (
        (mate, 0), (mate, 1), (turned(z, 2, nz), c), (turned(z, nz - 2, nz), c)
    ):
        pl.semaphore_signal(
            barrier, inc=1, device_id=there(chip, core, at_z), device_id_type=MESH
        )

    def left(ref, sem):
        remote(ref, ref, sem, sem, there(chip, 1 - c)).wait_send()

    def arrived(ref, sem):
        remote(ref, ref, sem, sem, there(chip, 1 - c)).wait_recv()

    inputs = []
    for h in range(2):
        half = pl.ds(h * HALF, HALF)
        inputs.append(
            [
                pltpu.make_async_copy(a.at[:, half], b.at[:, half], in_sem.at[h, n])
                for n, (a, b) in enumerate(
                    (
                        (g_in, g_ref), (q_in, q_ref), (k_in, k_ref),
                        (v_in, v_ref), (cot_in, cot_ref),
                    )
                )
            ]
        )
    for copies in inputs:
        for copy in copies:
            copy.start()

    def remote(src, dst, ss, rs, device):
        return pltpu.make_async_remote_copy(
            src_ref=src, dst_ref=dst, send_sem=ss, recv_sem=rs, device_id=device, device_id_type=MESH
        )

    row = lax.broadcasted_iota(jnp.int32, (BLOCK, BLOCK), 0)
    col = lax.broadcasted_iota(jnp.int32, (BLOCK, BLOCK), 1)
    left_half = lax.broadcasted_iota(jnp.int32, (64, 128), 1) < 64
    lane = lax.broadcasted_iota(jnp.int32, (BLOCK, 128), 1)
    mask0 = jnp.where(lane < 64, 1.0, 0.0).astype(BF16)
    mask1 = jnp.where(lane < 64, 0.0, 1.0).astype(BF16)
    upto = jnp.where(row >= col, 1.0, 0.0).astype(BF16)
    onward = jnp.where(row <= col, 1.0, 0.0).astype(BF16)

    def diagonal(m):
        return jnp.where(left_half, m[:64], m[64:])

    def pair_at(k):
        return lax.rem(k, 2) + 4 * lax.rem(lax.div(k, 2), 2) + 2 * lax.div(k, 4)

    def local_states(p, _):
        at = lanes(p * 128, 128)
        gate = g_ref[:, at]
        running = nn(upto, gate)
        exclusive = running - gate.astype(F32)
        run_s[:, at] = running
        end = jnp.exp(running[BLOCK - 1 : BLOCK])
        end_s[1, :, at] = jnp.broadcast_to(end, (8, 128))
        query = q_ref[:, at].astype(F32) * HEAD_DIM ** (-0.5)
        key = k_ref[:, at].astype(F32)
        qf = (query * jnp.exp(running)).astype(BF16)
        kf = (key * jnp.exp(-running)).astype(BF16)
        qb = (query * jnp.exp(-exclusive)).astype(BF16)
        kb = (key * jnp.exp(exclusive)).astype(BF16)
        qf_s[:, at] = qf
        kf_s[:, at] = kf
        qb_s[:, at] = qb
        kb_s[:, at] = kb
        value = v_ref[:, at]
        cot = cot_ref[:, at]
        uh = diagonal(tn(value, kf))
        wb = diagonal(tn(cot, qb))
        raw_s[2 * p] = uh
        raw_s[2 * p + 1] = wb
        place = 2 * pair_at(p)
        loc_s[1, 0, place] = (uh * end).astype(BF16)
        loc_s[1, 0, place + 1] = (wb * end).astype(BF16)
        loc_s[1, 1, place] = diagonal(tn(cot, qf)).astype(BF16)
        loc_s[1, 1, place + 1] = diagonal(tn(value, kb)).astype(BF16)
        return 0

    for h, copies in enumerate(inputs):
        for copy in copies:
            copy.wait()
        lax.fori_loop(h * (PAIRS // 2), (h + 1) * (PAIRS // 2), local_states, 0, unroll=UNROLL)

    pl.semaphore_wait(barrier, greeted + 5)

    lead = 1 - lax.rem(z, 2)
    follow = 1 - lead
    quarter = CHUNKS // 4

    def state_copies():
        return (
            remote(loc_s.at[1, lead], loc_s.at[0, lead], loc_ss.at[0], loc_rs.at[0], there(chip, 1 - c)),
            remote(end_s.at[1], end_s.at[0], loc_ss.at[1], loc_rs.at[1], there(chip, 1 - c)),
        )

    remote(
        end_s.at[1], fend_s.at[c], fend_ss, fend_rs.at[c], there(chip, 1, mate)
    ).start()
    for n in range(4):
        part = pl.ds(n * quarter, quarter)
        remote(
            loc_s.at[1, follow, part], fol_s.at[c, part], fol_ss, fol_rs.at[c, n],
            there(chip, 1, mate),
        ).start()

    @pl.when(c == 0)
    def _():
        for copy in state_copies():
            copy.start()

    for half in range(2):
        columns = pl.ds(half * HALF, HALF)
        mine = wv_s.at[half, chip, pl.ds(pl.multiple_of(c * 64, 64), 64), :]

        @pl.when(c == 0)
        def _():
            pltpu.make_async_copy(w_ref.at[:, columns], mine, w_loc).start()

        @pl.when(c == 1)
        def _():
            remote(w_ref.at[:, columns], mine, w0_ss, w0_rs, there(chip, 0)).start()

    w_shard = wv_s.at[:, chip, pl.ds(0, 64), :]

    x_slot = (xx * 2 + c, yy * 2 + c)

    def x_copies(role, i):
        if role == 0:
            to = turned(xx, i, nq)
            target = there(yy * nq + to, 0)
            pieces = [
                (
                    x_ref.at[:, lanes((b * nq + to) * 128, 128)],
                    xg_s.at[x_slot[0], :, pl.ds(b * 128, 128)],
                )
                for b in range(nq)
            ]
        else:
            to = turned(yy, i, nq)
            target = there(to * nq + xx, 1)
            pieces = [(x_ref.at[:, lanes(to * nq * 128, nq * 128)], xg_s.at[x_slot[1]])]
        return target, pieces

    def send_x(role, i):
        target, pieces = x_copies(role, i)

        def away():
            for src, dst in pieces:
                remote(src, dst, x_ss, x_rs, target).start()

        def at_home():
            for src, dst in pieces:
                pltpu.make_async_copy(src, dst, x_rs).start()

        if i == 0:
            pl.when(c != role)(away)
            pl.when(c == role)(at_home)
        else:
            away()

    for role in range(2):
        for i in range(nq):
            send_x(role, i)

    def chip_in(half, a, b):
        return b * nq + a if half == 0 else a * nq + b

    w_at = ((xx, yy), (yy, xx))

    def w_first():
        pltpu.make_async_copy(w_shard, w_shard, w_loc).wait()
        arrived(w_shard, w0_rs)
        for half, (a, b) in enumerate(w_at):
            for i in range(1, nq):
                remote(
                    wv_s.at[half, chip], wv_s.at[half, chip], w1_ss, w1_rs.at[half],
                    there(chip_in(half, turned(a, i, nq), b), 0),
                ).start()

    def both(a):
        return jnp.concatenate([a * mask0, a * mask1], axis=0)

    row2 = lax.broadcasted_iota(jnp.int32, (BLOCK, 256), 0)
    col2 = lax.rem(lax.broadcasted_iota(jnp.int32, (BLOCK, 256), 1), 128)
    lower = row2 >= col2
    upper = row2 <= col2

    def own_part(p, _):
        at = lanes(p * 128, 128)
        value = v_ref[:, at]
        cot = cot_ref[:, at]
        qf, kf, qb, kb = qf_s[:, at], kf_s[:, at], qb_s[:, at], kb_s[:, at]
        value2, cot2 = both(value), both(cot)
        qf2, kf2, qb2, kb2 = both(qf), both(kf), both(qb), both(kb)
        d_score = nt(cot, value2)
        d_score_t = nt(value, cot2)
        score_t = jnp.where(upper, nt(kf, qf2), 0.0) + jnp.where(lower, nt(kb, qb2), 0.0)
        dqf_s[:, at] = nn(jnp.where(lower, d_score, 0.0).astype(BF16), kf2)
        dqb_s[:, at] = nn(jnp.where(upper, d_score, 0.0).astype(BF16), kb2)
        dkf_s[:, at] = nn(jnp.where(upper, d_score_t, 0.0).astype(BF16), qf2)
        dkb_s[:, at] = nn(jnp.where(lower, d_score_t, 0.0).astype(BF16), qb2)
        dv_s[:, at] = nn(score_t.astype(BF16), cot2)
        return 0

    def own_parts():
        lax.fori_loop(0, PAIRS, own_part, 0, unroll=UNROLL)

    def turn_inputs():
        arrived(xg_s, x_rs)
        for slot in range(2 * nq):
            for b in range(nq):
                xgt_s[b, :, slot * BLOCK : (slot + 1) * BLOCK] = xg_s[
                    slot, :, b * 128 : (b + 1) * 128
                ].T

    def w_second():
        for half, (a, b) in enumerate(w_at):
            arrived(wv_s.at[0, pl.ds(0, nq - 1)], w1_rs.at[half])
            for i in range(1, nq):
                for j in range(nq):
                    block = wv_s.at[half, chip_in(half, j, b)]
                    remote(
                        block, block, w2_ss, w2_rs,
                        there(chip_in(half, a, turned(b, i, nq)), 0),
                    ).start()

    def before(way):
        return z + way * (nz - 1 - 2 * z)

    for way in range(2):

        @pl.when(before(way) == 0)
        def _():
            state_s[:, way] = jnp.zeros((2, *state_s.shape[2:]), BF16)

    @pl.when(before(lead) == 1)
    def _():
        in_s[...] = jnp.zeros(in_s.shape, BF16)

    def onward_copy(s, i):
        return remote(
            out_s.at[s, i], in_s.at[s, i], chain_ss.at[s], chain_rs.at[s, i],
            there(chip, 1, lax.rem(z + 2 - 4 * lead + nz, nz)),
        )

    def hand_copy(s, i, way):
        return remote(
            in_s.at[s, i], state_s.at[s, way, i], hand_ss.at[s], hand_rs.at[s, i],
            there(chip, 1, mate),
        )

    def forward_copy(way, i):
        return remote(
            state_s.at[0, way, i], state_s.at[1, way, i],
            fw_ss.at[way], fw_rs.at[lax.div(i, CHUNKS // 2), way], there(chip, 1 - c),
        )

    edge = jnp.minimum(z, nz - 1 - z)
    first = jnp.where(edge >= nz // 4, lead, lax.div(2 * z, nz))
    steps = 2 * CHUNKS
    own_first = CHUNKS // 2

    def taken(index):
        theirs = jnp.where((index >= own_first) & (index < own_first + CHUNKS), 1, 0)
        i = index - jnp.where(index < own_first, 0, jnp.where(theirs == 1, own_first, CHUNKS))
        return 1 - theirs, i

    def lead_step(index, _):
        s, i = taken(index)
        onward = onward_copy(s, i)

        @pl.when(index == 0)
        def _():
            arrived(fend_s.at[1], fend_rs.at[1])

        @pl.when(index == own_first)
        def _():
            arrived(fend_s.at[0], fend_rs.at[0])
            for copy in state_copies():
                copy.wait_recv()

        @pl.when(lax.rem(i, quarter) == 0)
        def _():
            arrived(fol_s.at[0, pl.ds(0, quarter)], fol_rs.at[s, lax.div(i, quarter)])

        @pl.when(before(lead) > 1)
        def _():
            onward.wait_recv()

        at = lanes(pair_at(lax.div(i, 2)) * 128, 128)
        state = in_s[s, i].astype(F32) * fend_s[s, 0:1, at] + fol_s[s, i].astype(F32)
        state_s[s, lead, i] = state.astype(BF16)

        @pl.when(before(lead) < nz - 1)
        def _():
            behind = state * end_s[s, 0:1, at] + loc_s[s, lead, i].astype(F32)
            out_s[s, i] = behind.astype(BF16)
            onward.start()

        @pl.when(before(lead) > 1)
        def _():
            hand_copy(s, i, lead).start()

        @pl.when(s == 0)
        def _():
            forward_copy(lead, i).start()

        return 0

    def follow_step(index, _):
        s, i = taken(index)
        hand_copy(s, i, follow).wait_recv()

        @pl.when(s == 0)
        def _():
            forward_copy(follow, i).start()

        return 0

    def chain(way, begin, end):
        @pl.when((c == 1) & (way == lead))
        def _():
            lax.fori_loop(begin, end, lead_step, 0)

        @pl.when((c == 1) & (way != lead) & (before(follow) > 0))
        def _():
            lax.fori_loop(begin, end, follow_step, 0)

    pl.when(c == 0)(w_first)
    pl.when((c == 0) | (edge >= nz // 4))(own_parts)
    chain(first, 0, steps)
    pl.when((c == 1) & (edge < nz // 4))(own_parts)
    pl.when(c == 0)(w_second)
    pl.when((c == 0) | (edge < 2))(turn_inputs)

    def spread(state):
        zero = jnp.zeros_like(state)
        return jnp.concatenate(
            [jnp.where(left_half, state, zero), jnp.where(left_half, zero, state)], axis=0
        ).astype(BF16)

    def value_part(i, _):
        p = pair_at(i)
        at = lanes(p * 128, 128)
        e2 = spread(state_s[1, 1, 2 * i].astype(F32) * end_s[1, 0:1, at])
        f2 = spread(state_s[1, 0, 2 * i + 1].astype(F32))
        dvb_s[:, at] = (dv_s[:, at] + nt(kf_s[:, at], e2) + nt(kb_s[:, at], f2)).astype(BF16)
        return 0

    def w_swap():
        arrived(wv_s.at[:, pl.ds(0, (nq - 1) * nq)], w2_rs)
        remote(wv_s, wv_s, w3_ss, w3_rs, there(chip, 1)).start()

    def send_dv(h, role, i):
        if role == 0:
            target = there(yy * nq + turned(xx, i, nq), 0)
        else:
            target = there(turned(yy, i, nq) * nq + xx, 1)
        src = dvb_s.at[:, pl.ds(role * HALF + h * 256, 256)]
        dst = dvg_s.at[h, x_slot[role]]

        def away():
            remote(src, dst, dv_ss, dv_rs.at[h], target).start()

        def at_home():
            pltpu.make_async_copy(src, dst, dv_rs.at[h]).start()

        if i == 0:
            pl.when(c != role)(away)
            pl.when(c == role)(at_home)
        else:
            away()

    def back(h):
        for way in range(2):

            @pl.when((c == 0) & (before(way) > 0))
            def _():
                arrived(state_s.at[1, way, pl.ds(0, CHUNKS // 2)], fw_rs.at[h, way])

    for h in range(2):
        chain(1 - first, h * CHUNKS, (h + 1) * CHUNKS)
        back(h)
        lax.fori_loop(
            h * (PAIRS // 2), (h + 1) * (PAIRS // 2), value_part, 0, unroll=UNROLL
        )
        for i in (2, 1, 3, 0) if nq == 4 else (1, 0):
            for role in range(2):
                send_dv(h, role, i)

    def finish(p, _):
        at = lanes(p * 128, 128)
        value = v_ref[:, at]
        cot = cot_ref[:, at]
        qf, kf, qb, kb = qf_s[:, at], kf_s[:, at], qb_s[:, at], kb_s[:, at]
        end = end_s[1, 0:1, at]
        place = 2 * pair_at(p)
        h_state = state_s[1, 0, place].astype(F32)
        f_state = state_s[1, 0, place + 1].astype(F32)
        e_state = (state_s[1, 1, place].astype(F32) * end).astype(BF16).astype(F32)
        r_state = (state_s[1, 1, place + 1].astype(F32) * end).astype(BF16).astype(F32)
        carry = jnp.sum(
            e_state * (h_state + raw_s[2 * p]) + r_state * (f_state + raw_s[2 * p + 1]),
            axis=0,
            keepdims=True,
        )
        h2, f2, e2, r2 = spread(h_state), spread(f_state), spread(e_state), spread(r_state)
        dqf = dqf_s[:, at] + nn(cot, h2)
        dqb = dqb_s[:, at] + nn(cot, r2)
        dkf = dkf_s[:, at] + nn(value, e2)
        dkb = dkb_s[:, at] + nn(value, f2)
        running = run_s[:, at]
        exclusive = running - g_ref[:, at].astype(F32)
        dq = (jnp.exp(running) * dqf + jnp.exp(-exclusive) * dqb) * HEAD_DIM ** (-0.5)
        dk = jnp.exp(-running) * dkf + jnp.exp(exclusive) * dkb
        dq_ref[:, at] = dq.astype(BF16)
        dk_ref[:, at] = dk.astype(BF16)
        fwd = qf.astype(F32) * dqf - kf.astype(F32) * dkf
        bwd = kb.astype(F32) * dkb - qb.astype(F32) * dqb
        both_ways = fwd + bwd
        high = both_ways.astype(BF16)
        low = (both_ways - high.astype(F32)).astype(BF16)
        dg = nn(onward, high) + nn(onward, low) - bwd + carry
        dg_ref[:, at] = dg.astype(BF16)
        return 0

    pl.when((c == 1) & (edge >= 2))(turn_inputs)
    pl.when(c == 0)(w_swap)
    lax.fori_loop(0, PAIRS, finish, 0, unroll=UNROLL)

    outputs = [
        pltpu.make_async_copy(a, b, out_sem.at[n])
        for n, (a, b) in enumerate(
            ((dq_ref, dq_out), (dk_ref, dk_out), (dg_ref, dg_out), (gi_ref, gi_out))
        )
    ]
    for copy in outputs[:3]:
        copy.start()

    tokens = 2 * nq * BLOCK

    def s2_copies(h):
        return [
            remote(
                pb_s.at[h, turned(pb, i, nq)], s2_s.at[h, i - 1],
                s2_ss.at[h], s2_rs.at[h],
                there(chip_at(pa, turned(pb, i, nq)), c),
            )
            for i in range(1, nq)
        ]

    for h in range(2):
        arrived(dvg_s.at[h], dv_rs.at[h])
        gathered = dvg_s[h].reshape(tokens, 256)
        for b in range(nq):
            part = nn(xgt_s[b], gathered)
            part_s[h, b] = part
            pb_s[h, b] = part.astype(BF16)
        for copy in s2_copies(h):
            copy.start()

    wide = 4 if nz == 16 else 2
    stack = nz // wide
    height = 128 // stack
    chunk = HALF // wide

    def z_copy(to):
        return remote(zb_s.at[to], zr_s.at[z], zr_ss, zr_rs, there(chip, c, to))

    for h in range(2):
        total = part_s[h, pb]
        left(s2_s.at[h], s2_ss.at[h])
        arrived(s2_s.at[h], s2_rs.at[h])
        for i in range(nq - 1):
            total = total + s2_s[h, i].astype(F32)
        per = wide // 2
        for r in range(stack):
            for l in range(per):
                zb_s[r * wide + h * per + l] = total[
                    r * height : (r + 1) * height, l * chunk : (l + 1) * chunk
                ].astype(BF16)
        for r in (2, 1, 3, 0) if stack == 4 else (1, 0):
            group_at = lax.rem(lax.div(z, wide) + r, stack)
            for l in range(per):
                to = group_at * wide + h * per + l
                pl.when(to != z)(lambda: z_copy(to).start())

    zr_s[z] = zb_s[z]

    left(zr_s.at[pl.ds(0, nz - 1)], zr_ss)
    arrived(zr_s.at[pl.ds(0, nz - 1)], zr_rs)
    rb_s[...] = jnp.sum(zr_s[...].astype(F32), axis=0).astype(BF16)

    owner = lax.div(2 * z, nz)
    slot = c * (nz // 2) + lax.rem(z, nz // 2)

    def out_copy(i):
        return remote(
            rb_s, gr_s.at[slot], za_ss, za_rs, there(chip, owner, turned(z, i, nz))
        )

    home = pltpu.make_async_copy(rb_s, gr_s.at[slot], za_rs)
    for near in range(nz // 2):
        out_copy(nz // 2 - near).start()
        if near > 0:
            out_copy(nz // 2 + near).start()
    pl.when(owner == c)(lambda: home.start())
    pl.when(owner != c)(lambda: out_copy(0).start())

    pl.when(c == 1)(lambda: arrived(wv_s, w3_rs))
    group = nq * 128
    for i in range(nq):
        low_half = wv_s[0, i * nq : (i + 1) * nq].reshape(group, HALF)
        high_half = wv_s[1, i * nq : (i + 1) * nq].reshape(group, HALF)
        gi_ref[:, i * group : (i + 1) * group] = (
            nt(dvb_s[:, :HALF], low_half) + nt(dvb_s[:, HALF:], high_half)
        ).astype(BF16)

    outputs[3].start()

    arrived(gr_s, za_rs)

    for copy in outputs:
        copy.wait()
    pl.when(owner == c)(lambda: left(zr_s.at[pl.ds(0, nz - 1)], za_ss))
    pl.when(owner != c)(lambda: left(zr_s, za_ss))

    @pl.when(c == 0)
    def _():
        for copy in state_copies():
            copy.wait_send()

    left(end_s.at[1], fend_ss)
    left(fol_s.at[0], fol_ss)

    @pl.when((c == 1) & (before(lead) < nz - 1))
    def _():
        for s in range(2):
            left(out_s.at[s], chain_ss.at[s])

    @pl.when((c == 1) & (before(lead) > 1))
    def _():
        for s in range(2):
            left(in_s.at[s], hand_ss.at[s])

    for way in range(2):

        @pl.when((c == 1) & (before(way) > 0))
        def _():
            left(state_s.at[0, way], fw_ss.at[way])

    @pl.when(c == 0)
    def _():
        left(wv_s.at[:, pl.ds(0, nq - 1)], w1_ss)
        left(wv_s.at[:, pl.ds(0, (nq - 1) * nq)], w2_ss)
        left(wv_s, w3_ss)

    @pl.when(c == 1)
    def _():
        left(w_shard, w0_ss)

    left(xg_s.at[pl.ds(0, 2 * nq - 1)], x_ss)
    left(dvg_s.at[:, pl.ds(0, 2 * nq - 1)], dv_ss)


def store(wide, dq, dk, dg, gi, gr, dq_out, dk_out, dg_out, gi_out, gw_out, gw_s, sems):
    copies = [
        pltpu.make_async_copy(a, b, sems.at[n])
        for n, (a, b) in enumerate(((gi, gi_out), (dq, dq_out), (dk, dk_out), (dg, dg_out)))
    ]
    for copy in copies:
        copy.start()
    count, height, chunk = gr.shape
    for s in range(count):
        role, t = s // (count // 2), s % (count // 2)
        rows, columns = t // wide * height, role * HALF + t % wide * chunk
        gw_s[rows : rows + height, columns : columns + chunk] = gr[s].astype(F32)
    last = pltpu.make_async_copy(gw_s, gw_out, sems.at[4])
    last.start()
    for copy in (*copies, last):
        copy.wait()


def per_device(nz, nq, inputs, queries, keys, values, log_decay, cotangent, value_weight):
    model = inputs.shape[2]
    slots = 2 * nq
    wide = 4 if nz == 16 else 2
    chunk = (128 * wide // nz, HALF // wide)
    dma = pltpu.SemaphoreType.DMA
    vm = pltpu.VMEM
    shapes = [((BLOCK, WIDTH), BF16)] * 3 + [((BLOCK, model), BF16)]
    sums = ((nz, *chunk), BF16)
    weight = ((64, WIDTH), F32)
    in_vmem = pl.BlockSpec(memory_space=pltpu.VMEM)
    anywhere = pl.BlockSpec(memory_space=pl.ANY)
    outs = pl.pallas_call(
        functools.partial(kernel, nz, nq),
        out_shape=tuple(vm(*shape) for shape in (*shapes, sums)),
        in_specs=[anywhere] * 7,
        out_specs=[anywhere] * 5,
        scratch_shapes=[
            *[vm((BLOCK, WIDTH), BF16)] * 8,
            vm((BLOCK, model), BF16),
            vm((BLOCK, WIDTH), F32),
            vm((2, 8, WIDTH), F32),
            *[vm((BLOCK, WIDTH), BF16)] * 4,
            vm((2, 2, CHUNKS, 64, 128), BF16),
            vm((CHUNKS, 64, 128), F32),
            vm((2, CHUNKS, 64, 128), BF16),
            vm((2, 8, WIDTH), F32),
            vm((2, CHUNKS, 64, 128), BF16),
            vm((2, CHUNKS, 64, 128), BF16),
            vm((2, 2, CHUNKS, 64, 128), BF16),
            *[vm((BLOCK, WIDTH), F32)] * 5,
            vm((BLOCK, WIDTH), BF16),
            vm((2, nq * nq, 128, HALF), BF16),
            vm((slots, BLOCK, nq * 128), BF16),
            vm((nq, 128, slots * BLOCK), BF16),
            vm((2, slots, BLOCK, 256), BF16),
            vm((2, nq, 128, 256), F32),
            vm((2, nq, 128, 256), BF16),
            vm((2, nq - 1, 128, 256), BF16),
            vm(*sums),
            vm(*sums),
            vm(chunk, BF16),
            dma((2, 5)), dma((4,)),
            dma((2,)), dma((2, CHUNKS)),
            dma((2,)), dma((2, CHUNKS)),
            dma((2,)), dma((2, 2)),
            dma((2,)), dma((2,)),
            dma, dma((2, 4)),
            dma, dma((2,)),
            *[dma] * 4,
            dma((2,)),
            *[dma] * 7,
            dma((2,)),
            dma((2,)), dma((2,)),
            *[dma] * 4,
        ],
        compiler_params=pltpu.CompilerParams(
            collective_id=0, has_side_effects=True, vmem_limit_bytes=65_300_000
        ),
    )(
        queries[0], keys[0], values[0], log_decay[0], cotangent[0], inputs[0], value_weight
    )
    dq, dk, dg, gi, gw = pl.pallas_call(
        functools.partial(store, wide),
        out_shape=tuple(jax.ShapeDtypeStruct(*shape) for shape in (*shapes, weight)),
        in_specs=[anywhere] * 4 + [in_vmem],
        out_specs=[anywhere] * 5,
        scratch_shapes=[vm(*weight), dma((5,))],
        compiler_params=pltpu.CompilerParams(vmem_limit_bytes=1024 * 1024),
    )(*outs)
    return dq[None], dk[None], dg[None], gi[None], gw


def solution(mesh):
    nz = mesh.shape["sp"]
    nq = 4 if mesh.shape["dp"] == 32 else 2
    tokens = P("dp", "sp", None)
    return jax.shard_map(
        functools.partial(per_device, nz, nq),
        mesh=mesh,
        in_specs=(tokens,) * 6 + (P("dp", None),),
        out_specs=(tokens,) * 4 + (P("dp", None),),
        check_vma=False,
    )
```

time: 88.8 us -> 76.8 us (0.86)
  Pallas kernels: 88 us -> 75.9 us
    pallas_call x1, Pallas kernels: 86.8 us -> 74.7 us  [per_device(): pl.pallas_call(functools.partial(kernel, nz, nq), out_shape=tuple((vm(*sh...]
where the time goes in v3:
time: 76.8 us; the launch traced here: 76.6 us
  Pallas kernels  75.9 us (99%)
    pallas_call x1, Pallas kernels, per_device(): pl.pallas_call(functools.partial(kernel, nz, nq), out_shape=tuple((vm(*sh...  74.7 us

profile of v3, /device:TPU:1, one launch (start us, length us, event | category | flops | bytes accessed | tf_op | source)
XLA Modules:
  0.0 76.6 jit_solution(11237917110991848776)
XLA Ops:
  0.6 74.7 %shard_map.110 = (bf16[128,1024]{1,0:T(8,128)(2,1)S(1)}, bf16[128,1024]{1,0:T(8,128)(2,1)S(1)}, bf16[128,1024]{1,0:T(8,128)(2,1)S(1)}, bf16[128,2048]{1,0:T(8,128)(2,1)S(1)}, bf16[16,32,128]{2,1,0:T(8,128)(2,1)S(1)}) custom-call(bf16[128,1024]{1,0:T(8,128)(2,1)} %bitcast.11, bf16[128,1024]{1,0:T(8,128)(2,1)} %bitcast.12, bf16[128,1024]{1,0:T(8,128)(2,1)} %bitcast.13, ...), custom_call_target="tpu_custom_call" | custom-call | tf_op jit(solution)/shard_map/pallas_call | solution.py:678
  75.4 1.2 %shard_map.111 = (bf16[128,1024]{1,0:T(8,128)(2,1)}, bf16[128,1024]{1,0:T(8,128)(2,1)}, bf16[128,1024]{1,0:T(8,128)(2,1)}, bf16[128,2048]{1,0:T(8,128)(2,1)}, f32[64,1024]{1,0:T(8,128)}) custom-call(bf16[128,1024]{1,0:T(8,128)(2,1)S(1)} %get-tuple-element.15.dq, bf16[128,1024]{1,0:T(8,128)(2,1)S(1)} %get-tuple-element.16.dk, ...), custom_call_target="tpu_custom_call" | custom-call | tf_op jit(solution)/shard_map/pallas_call | solution.py:728

commit v4 on v3

--- a/solution.py
+++ b/solution.py
@@ -17,6 +17,7 @@
 CHUNKS = 2 * PAIRS
 HEAD_DIM = 64
 UNROLL = 2
+PARTS = 4
 
 
 def nn(a, b):
@@ -89,23 +90,11 @@
     def arrived(ref, sem):
         remote(ref, ref, sem, sem, there(chip, 1 - c)).wait_recv()
 
-    inputs = []
+    named = ((g_in, g_ref), (q_in, q_ref), (k_in, k_ref), (v_in, v_ref), (cot_in, cot_ref))
     for h in range(2):
-        half = pl.ds(h * HALF, HALF)
-        inputs.append(
-            [
-                pltpu.make_async_copy(a.at[:, half], b.at[:, half], in_sem.at[h, n])
-                for n, (a, b) in enumerate(
-                    (
-                        (g_in, g_ref), (q_in, q_ref), (k_in, k_ref),
-                        (v_in, v_ref), (cot_in, cot_ref),
-                    )
-                )
-            ]
-        )
-    for copies in inputs:
-        for copy in copies:
-            copy.start()
+        for n, (a, b) in enumerate(named):
+            for columns in (pl.ds(h * 256, 256), pl.ds(HALF + h * 256, 256)):
+                pltpu.make_async_copy(a.at[:, columns], b.at[:, columns], in_sem.at[h, n]).start()
 
     def remote(src, dst, ss, rs, device):
         return pltpu.make_async_remote_copy(
@@ -125,9 +114,13 @@
         return jnp.where(left_half, m[:64], m[64:])
 
     def pair_at(k):
-        return lax.rem(k, 2) + 4 * lax.rem(lax.div(k, 2), 2) + 2 * lax.div(k, 4)
-
-    def local_states(p, _):
+        return lax.div(k, 2) + (PAIRS // 2) * lax.rem(k, 2)
+
+    def place_of(p):
+        return 4 * lax.rem(p, PAIRS // 2) + 2 * lax.div(p, PAIRS // 2)
+
+    def local_states(k, _):
+        p = pair_at(k)
         at = lanes(p * 128, 128)
         gate = g_ref[:, at]
         running = nn(upto, gate)
@@ -151,44 +144,51 @@
         wb = diagonal(tn(cot, qb))
         raw_s[2 * p] = uh
         raw_s[2 * p + 1] = wb
-        place = 2 * pair_at(p)
+        place = 2 * k
         loc_s[1, 0, place] = (uh * end).astype(BF16)
         loc_s[1, 0, place + 1] = (wb * end).astype(BF16)
         loc_s[1, 1, place] = diagonal(tn(cot, qf)).astype(BF16)
         loc_s[1, 1, place + 1] = diagonal(tn(value, kb)).astype(BF16)
         return 0
 
-    for h, copies in enumerate(inputs):
-        for copy in copies:
-            copy.wait()
-        lax.fori_loop(h * (PAIRS // 2), (h + 1) * (PAIRS // 2), local_states, 0, unroll=UNROLL)
-
-    pl.semaphore_wait(barrier, greeted + 5)
-
     lead = 1 - lax.rem(z, 2)
     follow = 1 - lead
-    quarter = CHUNKS // 4
-
-    def state_copies():
-        return (
-            remote(loc_s.at[1, lead], loc_s.at[0, lead], loc_ss.at[0], loc_rs.at[0], there(chip, 1 - c)),
-            remote(end_s.at[1], end_s.at[0], loc_ss.at[1], loc_rs.at[1], there(chip, 1 - c)),
-        )
-
-    remote(
-        end_s.at[1], fend_s.at[c], fend_ss, fend_rs.at[c], there(chip, 1, mate)
-    ).start()
-    for n in range(4):
-        part = pl.ds(n * quarter, quarter)
-        remote(
-            loc_s.at[1, follow, part], fol_s.at[c, part], fol_ss, fol_rs.at[c, n],
-            there(chip, 1, mate),
-        ).start()
-
-    @pl.when(c == 0)
-    def _():
-        for copy in state_copies():
-            copy.start()
+    quarter = CHUNKS // PARTS
+    group = CHUNKS // 2
+
+    def end_columns(h):
+        return (pl.ds(h * 256, 256), pl.ds(HALF + h * 256, 256))
+
+    for h in range(2):
+        for n, (a, b) in enumerate(named):
+            pltpu.make_async_copy(a.at[:, pl.ds(0, HALF)], b.at[:, pl.ds(0, HALF)], in_sem.at[h, n]).wait()
+        lax.fori_loop(h * (PAIRS // 2), (h + 1) * (PAIRS // 2), local_states, 0, unroll=UNROLL)
+        if h == 0:
+            pl.semaphore_wait(barrier, greeted + 5)
+        for columns in end_columns(h):
+            remote(
+                end_s.at[1, :, columns], fend_s.at[c, :, columns], fend_ss, fend_rs.at[c, h],
+                there(chip, 1, mate),
+            ).start()
+        for n in range(h * PARTS // 2, (h + 1) * PARTS // 2):
+            part = pl.ds(n * quarter, quarter)
+            remote(
+                loc_s.at[1, follow, part], fol_s.at[c, part], fol_ss, fol_rs.at[c, n],
+                there(chip, 1, mate),
+            ).start()
+
+        @pl.when(c == 0)
+        def _():
+            for columns in end_columns(h):
+                remote(
+                    end_s.at[1, :, columns], end_s.at[0, :, columns],
+                    loc_ss.at[1], loc_rs.at[1, h], there(chip, 1),
+                ).start()
+            part = pl.ds(h * group, group)
+            remote(
+                loc_s.at[1, lead, part], loc_s.at[0, lead, part],
+                loc_ss.at[0], loc_rs.at[0, h], there(chip, 1),
+            ).start()
 
     for half in range(2):
         columns = pl.ds(half * HALF, HALF)
@@ -291,7 +291,7 @@
         arrived(xg_s, x_rs)
         for slot in range(2 * nq):
             for b in range(nq):
-                xgt_s[b, :, slot * BLOCK : (slot + 1) * BLOCK] = xg_s[
+                xgt_s[b * 128 : (b + 1) * 128, slot * BLOCK : (slot + 1) * BLOCK] = xg_s[
                     slot, :, b * 128 : (b + 1) * 128
                 ].T
 
@@ -334,32 +334,32 @@
     def forward_copy(way, i):
         return remote(
             state_s.at[0, way, i], state_s.at[1, way, i],
-            fw_ss.at[way], fw_rs.at[lax.div(i, CHUNKS // 2), way], there(chip, 1 - c),
+            fw_ss.at[way], fw_rs.at[lax.div(i, quarter), way], there(chip, 1 - c),
         )
 
     edge = jnp.minimum(z, nz - 1 - z)
     first = jnp.where(edge >= nz // 4, lead, lax.div(2 * z, nz))
     steps = 2 * CHUNKS
-    own_first = CHUNKS // 2
 
     def taken(index):
-        theirs = jnp.where((index >= own_first) & (index < own_first + CHUNKS), 1, 0)
-        i = index - jnp.where(index < own_first, 0, jnp.where(theirs == 1, own_first, CHUNKS))
-        return 1 - theirs, i
+        part = lax.div(index, 2 * quarter)
+        rest = lax.rem(index, 2 * quarter)
+        s = 1 - lax.rem(part + lax.div(rest, quarter), 2)
+        return s, part * quarter + lax.rem(rest, quarter)
 
     def lead_step(index, _):
         s, i = taken(index)
         onward = onward_copy(s, i)
 
-        @pl.when(index == 0)
-        def _():
-            arrived(fend_s.at[1], fend_rs.at[1])
-
-        @pl.when(index == own_first)
-        def _():
-            arrived(fend_s.at[0], fend_rs.at[0])
-            for copy in state_copies():
-                copy.wait_recv()
+        @pl.when(lax.rem(i, group) == 0)
+        def _():
+            half = lax.div(i, group)
+            arrived(fend_s.at[0, :, pl.ds(0, HALF)], fend_rs.at[s, half])
+
+            @pl.when(s == 0)
+            def _():
+                arrived(end_s.at[0, :, pl.ds(0, HALF)], loc_rs.at[1, half])
+                arrived(loc_s.at[0, lead, pl.ds(0, group)], loc_rs.at[0, half])
 
         @pl.when(lax.rem(i, quarter) == 0)
         def _():
@@ -438,7 +438,7 @@
             target = there(yy * nq + turned(xx, i, nq), 0)
         else:
             target = there(turned(yy, i, nq) * nq + xx, 1)
-        src = dvb_s.at[:, pl.ds(role * HALF + h * 256, 256)]
+        src = dvb_s.at[:, pl.ds(role * HALF + h * 128, 128)]
         dst = dvg_s.at[h, x_slot[role]]
 
         def away():
@@ -458,14 +458,12 @@
 
             @pl.when((c == 0) & (before(way) > 0))
             def _():
-                arrived(state_s.at[1, way, pl.ds(0, CHUNKS // 2)], fw_rs.at[h, way])
-
-    for h in range(2):
-        chain(1 - first, h * CHUNKS, (h + 1) * CHUNKS)
+                arrived(state_s.at[1, way, pl.ds(0, quarter)], fw_rs.at[h, way])
+
+    for h in range(PARTS):
+        chain(1 - first, 2 * h * quarter, 2 * (h + 1) * quarter)
         back(h)
-        lax.fori_loop(
-            h * (PAIRS // 2), (h + 1) * (PAIRS // 2), value_part, 0, unroll=UNROLL
-        )
+        lax.fori_loop(2 * h, 2 * h + 2, value_part, 0, unroll=2)
         for i in (2, 1, 3, 0) if nq == 4 else (1, 0):
             for role in range(2):
                 send_dv(h, role, i)
@@ -476,7 +474,7 @@
         cot = cot_ref[:, at]
         qf, kf, qb, kb = qf_s[:, at], kf_s[:, at], qb_s[:, at], kb_s[:, at]
         end = end_s[1, 0:1, at]
-        place = 2 * pair_at(p)
+        place = place_of(p)
         h_state = state_s[1, 0, place].astype(F32)
         f_state = state_s[1, 0, place + 1].astype(F32)
         e_state = (state_s[1, 1, place].astype(F32) * end).astype(BF16).astype(F32)
@@ -531,50 +529,49 @@
             for i in range(1, nq)
         ]
 
-    for h in range(2):
+    for h in range(PARTS):
         arrived(dvg_s.at[h], dv_rs.at[h])
-        gathered = dvg_s[h].reshape(tokens, 256)
-        for b in range(nq):
-            part = nn(xgt_s[b], gathered)
-            part_s[h, b] = part
-            pb_s[h, b] = part.astype(BF16)
+        part = nn(xgt_s[...], dvg_s[h].reshape(tokens, 128))
+        part_s[h] = part.reshape(nq, 128, 128)
+        pb_s[h] = part.astype(BF16).reshape(nq, 128, 128)
         for copy in s2_copies(h):
             copy.start()
 
-    wide = 4 if nz == 16 else 2
+    wide = PARTS
     stack = nz // wide
     height = 128 // stack
-    chunk = HALF // wide
+
+    per = stack // 2
+
+    def summing(r, part):
+        if r < per:
+            return nz // 2 + part * per + r
+        return (PARTS - 1 - part) * per + r - per
 
     def z_copy(to):
         return remote(zb_s.at[to], zr_s.at[z], zr_ss, zr_rs, there(chip, c, to))
 
-    for h in range(2):
+    for h in range(PARTS):
         total = part_s[h, pb]
-        left(s2_s.at[h], s2_ss.at[h])
         arrived(s2_s.at[h], s2_rs.at[h])
         for i in range(nq - 1):
             total = total + s2_s[h, i].astype(F32)
-        per = wide // 2
         for r in range(stack):
-            for l in range(per):
-                zb_s[r * wide + h * per + l] = total[
-                    r * height : (r + 1) * height, l * chunk : (l + 1) * chunk
-                ].astype(BF16)
-        for r in (2, 1, 3, 0) if stack == 4 else (1, 0):
-            group_at = lax.rem(lax.div(z, wide) + r, stack)
-            for l in range(per):
-                to = group_at * wide + h * per + l
-                pl.when(to != z)(lambda: z_copy(to).start())
+            zb_s[summing(r, h)] = total[r * height : (r + 1) * height].astype(BF16)
+        for r in range(stack):
+            to = summing(r, h)
+            pl.when(to != z)(lambda: z_copy(to).start())
 
     zr_s[z] = zb_s[z]
 
-    left(zr_s.at[pl.ds(0, nz - 1)], zr_ss)
     arrived(zr_s.at[pl.ds(0, nz - 1)], zr_rs)
     rb_s[...] = jnp.sum(zr_s[...].astype(F32), axis=0).astype(BF16)
 
-    owner = lax.div(2 * z, nz)
-    slot = c * (nz // 2) + lax.rem(z, nz // 2)
+    upper_z = lax.div(2 * z, nz)
+    owner = 1 - upper_z
+    depth = lax.div(lax.rem(z, nz // 2), per)
+    part_here = depth * upper_z + (PARTS - 1 - depth) * (1 - upper_z)
+    slot = c * (nz // 2) + part_here * per + lax.rem(z, per)
 
     def out_copy(i):
         return remote(
@@ -604,13 +601,16 @@
 
     for copy in outputs:
         copy.wait()
+    left(zr_s.at[pl.ds(0, nz - 1)], zr_ss)
+    for h in range(PARTS):
+        left(s2_s.at[h], s2_ss.at[h])
     pl.when(owner == c)(lambda: left(zr_s.at[pl.ds(0, nz - 1)], za_ss))
     pl.when(owner != c)(lambda: left(zr_s, za_ss))
 
     @pl.when(c == 0)
     def _():
-        for copy in state_copies():
-            copy.wait_send()
+        left(loc_s.at[1, lead], loc_ss.at[0])
+        left(end_s.at[1], loc_ss.at[1])
 
     left(end_s.at[1], fend_ss)
     left(fol_s.at[0], fol_ss)
@@ -645,7 +645,7 @@
     left(dvg_s.at[:, pl.ds(0, 2 * nq - 1)], dv_ss)
 
 
-def store(wide, dq, dk, dg, gi, gr, dq_out, dk_out, dg_out, gi_out, gw_out, gw_s, sems):
+def store(dq, dk, dg, gi, gr, dq_out, dk_out, dg_out, gi_out, gw_out, gw_s, sems):
     copies = [
         pltpu.make_async_copy(a, b, sems.at[n])
         for n, (a, b) in enumerate(((gi, gi_out), (dq, dq_out), (dk, dk_out), (dg, dg_out)))
@@ -655,7 +655,8 @@
     count, height, chunk = gr.shape
     for s in range(count):
         role, t = s // (count // 2), s % (count // 2)
-        rows, columns = t // wide * height, role * HALF + t % wide * chunk
+        per = count // 2 // PARTS
+        rows, columns = t % per * height, role * HALF + t // per * chunk
         gw_s[rows : rows + height, columns : columns + chunk] = gr[s].astype(F32)
     last = pltpu.make_async_copy(gw_s, gw_out, sems.at[4])
     last.start()
@@ -666,7 +667,7 @@
 def per_device(nz, nq, inputs, queries, keys, values, log_decay, cotangent, value_weight):
     model = inputs.shape[2]
     slots = 2 * nq
-    wide = 4 if nz == 16 else 2
+    wide = PARTS
     chunk = (128 * wide // nz, HALF // wide)
     dma = pltpu.SemaphoreType.DMA
     vm = pltpu.VMEM
@@ -697,26 +698,26 @@
             vm((BLOCK, WIDTH), BF16),
             vm((2, nq * nq, 128, HALF), BF16),
             vm((slots, BLOCK, nq * 128), BF16),
-            vm((nq, 128, slots * BLOCK), BF16),
-            vm((2, slots, BLOCK, 256), BF16),
-            vm((2, nq, 128, 256), F32),
-            vm((2, nq, 128, 256), BF16),
-            vm((2, nq - 1, 128, 256), BF16),
+            vm((nq * 128, slots * BLOCK), BF16),
+            vm((PARTS, slots, BLOCK, 128), BF16),
+            vm((PARTS, nq, 128, 128), F32),
+            vm((PARTS, nq, 128, 128), BF16),
+            vm((PARTS, nq - 1, 128, 128), BF16),
             vm(*sums),
             vm(*sums),
             vm(chunk, BF16),
             dma((2, 5)), dma((4,)),
             dma((2,)), dma((2, CHUNKS)),
             dma((2,)), dma((2, CHUNKS)),
+            dma((2,)), dma((PARTS, 2)),
             dma((2,)), dma((2, 2)),
-            dma((2,)), dma((2,)),
-            dma, dma((2, 4)),
-            dma, dma((2,)),
+            dma, dma((2, PARTS)),
+            dma, dma((2, 2)),
             *[dma] * 4,
             dma((2,)),
             *[dma] * 7,
-            dma((2,)),
-            dma((2,)), dma((2,)),
+            dma((PARTS,)),
+            dma((PARTS,)), dma((PARTS,)),
             *[dma] * 4,
         ],
         compiler_params=pltpu.CompilerParams(
@@ -726,7 +727,7 @@
         queries[0], keys[0], values[0], log_decay[0], cotangent[0], inputs[0], value_weight
     )
     dq, dk, dg, gi, gw = pl.pallas_call(
-        functools.partial(store, wide),
+        store,
         out_shape=tuple(jax.ShapeDtypeStruct(*shape) for shape in (*shapes, weight)),
         in_specs=[anywhere] * 4 + [in_vmem],
         out_specs=[anywhere] * 5,

time: 76.8 us -> 71.8 us (0.935)
  Pallas kernels: 75.9 us -> 70.6 us
    pallas_call x1, Pallas kernels: 74.7 us -> 69.4 us  [per_device(): pl.pallas_call(functools.partial(kernel, nz, nq), out_shape=tuple((vm(*sh...]
where the time goes in v4:
time: 71.8 us; the launch traced here: 71.2 us
  Pallas kernels  70.6 us (98%)
    pallas_call x1, Pallas kernels, per_device(): pl.pallas_call(functools.partial(kernel, nz, nq), out_shape=tuple((vm(*sh...  69.4 us

profile of v4, /device:TPU:1, one launch (start us, length us, event | category | flops | bytes accessed | tf_op | source)
XLA Modules:
  0.0 71.2 jit_solution(14673906236667066620)
XLA Ops:
  0.6 69.4 %shard_map.110 = (bf16[128,1024]{1,0:T(8,128)(2,1)S(1)}, bf16[128,1024]{1,0:T(8,128)(2,1)S(1)}, bf16[128,1024]{1,0:T(8,128)(2,1)S(1)}, bf16[128,2048]{1,0:T(8,128)(2,1)S(1)}, bf16[16,32,128]{2,1,0:T(8,128)(2,1)S(1)}) custom-call(bf16[128,1024]{1,0:T(8,128)(2,1)} %bitcast.11, bf16[128,1024]{1,0:T(8,128)(2,1)} %bitcast.12, bf16[128,1024]{1,0:T(8,128)(2,1)} %bitcast.13, ...), custom_call_target="tpu_custom_call" | custom-call | tf_op jit(solution)/shard_map/pallas_call | solution.py:679
  70.0 1.2 %shard_map.111 = (bf16[128,1024]{1,0:T(8,128)(2,1)}, bf16[128,1024]{1,0:T(8,128)(2,1)}, bf16[128,1024]{1,0:T(8,128)(2,1)}, bf16[128,2048]{1,0:T(8,128)(2,1)}, f32[64,1024]{1,0:T(8,128)}) custom-call(bf16[128,1024]{1,0:T(8,128)(2,1)S(1)} %get-tuple-element.15.dq, bf16[128,1024]{1,0:T(8,128)(2,1)S(1)} %get-tuple-element.16.dk, ...), custom_call_target="tpu_custom_call" | custom-call | tf_op jit(solution)/shard_map/pallas_call | solution.py:729

commit v5 on v4

--- a/solution.py
+++ b/solution.py
@@ -16,7 +16,7 @@
 PAIRS = WIDTH // 128
 CHUNKS = 2 * PAIRS
 HEAD_DIM = 64
-UNROLL = 2
+UNROLL = 4
 PARTS = 4
 
 
@@ -92,9 +92,9 @@
 
     named = ((g_in, g_ref), (q_in, q_ref), (k_in, k_ref), (v_in, v_ref), (cot_in, cot_ref))
     for h in range(2):
-        for n, (a, b) in enumerate(named):
+        for a, b in named:
             for columns in (pl.ds(h * 256, 256), pl.ds(HALF + h * 256, 256)):
-                pltpu.make_async_copy(a.at[:, columns], b.at[:, columns], in_sem.at[h, n]).start()
+                pltpu.make_async_copy(a.at[:, columns], b.at[:, columns], in_sem.at[h]).start()
 
     def remote(src, dst, ss, rs, device):
         return pltpu.make_async_remote_copy(
@@ -156,12 +156,15 @@
     quarter = CHUNKS // PARTS
     group = CHUNKS // 2
 
+    def half_inputs():
+        return wv_s.at[0, pl.ds(0, 5)] if nq == 4 else xg_s.at[:, :, pl.ds(0, 128)]
+
     def end_columns(h):
         return (pl.ds(h * 256, 256), pl.ds(HALF + h * 256, 256))
 
     for h in range(2):
-        for n, (a, b) in enumerate(named):
-            pltpu.make_async_copy(a.at[:, pl.ds(0, HALF)], b.at[:, pl.ds(0, HALF)], in_sem.at[h, n]).wait()
+        taken_in = half_inputs()
+        pltpu.make_async_copy(taken_in, taken_in, in_sem.at[h]).wait()
         lax.fori_loop(h * (PAIRS // 2), (h + 1) * (PAIRS // 2), local_states, 0, unroll=UNROLL)
         if h == 0:
             pl.semaphore_wait(barrier, greeted + 5)
@@ -327,13 +330,14 @@
 
     def hand_copy(s, i, way):
         return remote(
-            in_s.at[s, i], state_s.at[s, way, i], hand_ss.at[s], hand_rs.at[s, i],
+            in_s.at[s, i], state_s.at[s, way, i], hand_ss.at[s], hand_rs.at[s, lax.div(i, quarter)],
             there(chip, 1, mate),
         )
 
-    def forward_copy(way, i):
+    def forward_copy(way, i, count=1):
+        part = pl.ds(i, count)
         return remote(
-            state_s.at[0, way, i], state_s.at[1, way, i],
+            state_s.at[0, way, part], state_s.at[1, way, part],
             fw_ss.at[way], fw_rs.at[lax.div(i, quarter), way], there(chip, 1 - c),
         )
 
@@ -390,12 +394,12 @@
         return 0
 
     def follow_step(index, _):
-        s, i = taken(index)
-        hand_copy(s, i, follow).wait_recv()
+        s, i = taken(index * quarter)
+        arrived(state_s.at[0, follow, pl.ds(0, quarter)], hand_rs.at[s, lax.div(i, quarter)])
 
         @pl.when(s == 0)
         def _():
-            forward_copy(follow, i).start()
+            forward_copy(follow, i, quarter).start()
 
         return 0
 
@@ -406,7 +410,7 @@
 
         @pl.when((c == 1) & (way != lead) & (before(follow) > 0))
         def _():
-            lax.fori_loop(begin, end, follow_step, 0)
+            lax.fori_loop(begin // quarter, end // quarter, follow_step, 0)
 
     pl.when(c == 0)(w_first)
     pl.when((c == 0) | (edge >= nz // 4))(own_parts)
@@ -529,14 +533,6 @@
             for i in range(1, nq)
         ]
 
-    for h in range(PARTS):
-        arrived(dvg_s.at[h], dv_rs.at[h])
-        part = nn(xgt_s[...], dvg_s[h].reshape(tokens, 128))
-        part_s[h] = part.reshape(nq, 128, 128)
-        pb_s[h] = part.astype(BF16).reshape(nq, 128, 128)
-        for copy in s2_copies(h):
-            copy.start()
-
     wide = PARTS
     stack = nz // wide
     height = 128 // stack
@@ -551,7 +547,7 @@
     def z_copy(to):
         return remote(zb_s.at[to], zr_s.at[z], zr_ss, zr_rs, there(chip, c, to))
 
-    for h in range(PARTS):
+    def reduce_part(h):
         total = part_s[h, pb]
         arrived(s2_s.at[h], s2_rs.at[h])
         for i in range(nq - 1):
@@ -561,6 +557,19 @@
         for r in range(stack):
             to = summing(r, h)
             pl.when(to != z)(lambda: z_copy(to).start())
+
+    for h in range(PARTS):
+        arrived(dvg_s.at[h], dv_rs.at[h])
+        part = nn(xgt_s[...], dvg_s[h].reshape(tokens, 128))
+        part_s[h] = part.reshape(nq, 128, 128)
+        pb_s[h] = part.astype(BF16).reshape(nq, 128, 128)
+        for copy in s2_copies(h):
+            copy.start()
+        if h >= 2:
+            reduce_part(h - 2)
+
+    reduce_part(PARTS - 2)
+    reduce_part(PARTS - 1)
 
     zr_s[z] = zb_s[z]
 
@@ -706,9 +715,9 @@
             vm(*sums),
             vm(*sums),
             vm(chunk, BF16),
-            dma((2, 5)), dma((4,)),
+            dma((2,)), dma((4,)),
             dma((2,)), dma((2, CHUNKS)),
-            dma((2,)), dma((2, CHUNKS)),
+            dma((2,)), dma((2, PARTS)),
             dma((2,)), dma((PARTS, 2)),
             dma((2,)), dma((2, 2)),
             dma, dma((2, PARTS)),

time: 71.8 us -> 72 us (level)
  no operation moved by 1% of the time
where the time goes in v5:
time: 72 us; the launch traced here: 71.3 us
  Pallas kernels  70.6 us (98%)
    pallas_call x1, Pallas kernels, per_device(): pl.pallas_call(functools.partial(kernel, nz, nq), out_shape=tuple((vm(*sh...  69.5 us

profile of v5, /device:TPU:1, one launch (start us, length us, event | category | flops | bytes accessed | tf_op | source)
XLA Modules:
  0.0 71.3 jit_solution(5591352479410311788)
XLA Ops:
  0.6 69.5 %shard_map.110 = (bf16[128,1024]{1,0:T(8,128)(2,1)S(1)}, bf16[128,1024]{1,0:T(8,128)(2,1)S(1)}, bf16[128,1024]{1,0:T(8,128)(2,1)S(1)}, bf16[128,2048]{1,0:T(8,128)(2,1)S(1)}, bf16[16,32,128]{2,1,0:T(8,128)(2,1)S(1)}) custom-call(bf16[128,1024]{1,0:T(8,128)(2,1)} %bitcast.11, bf16[128,1024]{1,0:T(8,128)(2,1)} %bitcast.12, bf16[128,1024]{1,0:T(8,128)(2,1)} %bitcast.13, ...), custom_call_target="tpu_custom_call" | custom-call | tf_op jit(solution)/shard_map/pallas_call | solution.py:688
  70.1 1.2 %shard_map.111 = (bf16[128,1024]{1,0:T(8,128)(2,1)}, bf16[128,1024]{1,0:T(8,128)(2,1)}, bf16[128,1024]{1,0:T(8,128)(2,1)}, bf16[128,2048]{1,0:T(8,128)(2,1)}, f32[64,1024]{1,0:T(8,128)}) custom-call(bf16[128,1024]{1,0:T(8,128)(2,1)S(1)} %get-tuple-element.15.dq, bf16[128,1024]{1,0:T(8,128)(2,1)S(1)} %get-tuple-element.16.dk, ...), custom_call_target="tpu_custom_call" | custom-call | tf_op jit(solution)/shard_map/pallas_call | solution.py:738
